TPU v7x, 128 devices: a whole 4x4x4 slice. The times are simulated.
128 devices in a mesh: rep: 16 (over z, x), fs: 4 (over y), tp: 2 (over core).
Axes of the slice: x: 4, y: 4, z: 4, core: 2. Of those that a mesh axis runs over, the one named last changes fastest.
Arguments:
- inputs: bfloat16 [64, 768, 2048], P(('rep', 'fs'), 'tp'), may hold values from -6 to 6
- pre_gate: bfloat16 [64, 768, 2816], P(('rep', 'fs'), None, 'tp'), may hold values from -6 to 6
- pre_up: bfloat16 [64, 768, 2816], P(('rep', 'fs'), None, 'tp'), may hold values from -6 to 6
- cotangent: bfloat16 [64, 768, 2816], P(('rep', 'fs'), None, 'tp'), may hold values from -16 to 16
- w_gate: bfloat16 [2048, 2816], P('fs', 'tp'), may hold values from -0.125 to 0.125
- w_up: bfloat16 [2048, 2816], P('fs', 'tp'), may hold values from -0.125 to 0.125
- taps_gate: bfloat16 [3, 2816], replicated, may hold values from -3 to 3
- taps_up: bfloat16 [3, 2816], replicated, may hold values from -3 to 3
Outputs:
- grad_inputs: bfloat16 [64, 768, 2048], P(('rep', 'fs'), 'tp')
- grad_w_gate: float32 [2048, 2816], P('fs', 'tp')
- grad_w_up: float32 [2048, 2816], P('fs', 'tp')
- grad_taps_gate: float32 [3, 2816], replicated
- grad_taps_up: float32 [3, 2816], replicated
All inputs are finite; a program needn't handle non-finite values.
Results may differ from a plain program's by a relative error of at most 0.0059.
Values may be sent and summed in bfloat16 or wider, within the bound.
No kernel may reach another device: no remote copies, remote signals or barrier semaphores. Data moves between devices by JAX's collectives and lax.ppermute only.
A program may use at most 192 MiB of HBM per device.

v0:
```python
import functools

import jax
import jax.numpy as jnp
from jax import lax
from jax.experimental import pallas as pl
from jax.experimental.pallas import tpu as pltpu
from jax.sharding import PartitionSpec as P


SIDE = 4
HOPS = (1, 3, 2)
LANES = 128
CHUNK = 32
HALO = 8
GROUPS = ((6, "zx"), (5, "xz"))
DIMS = {"y": 0, "z": 1, "x": 2}


def shift(value, axis, hop):
    ring = range(SIDE)
    if axis == "y":
        return lax.ppermute(value, "fs", [(i, (i + hop) % SIDE) for i in ring])
    if axis == "z":
        pairs = [(z * SIDE + x, (z + hop) % SIDE * SIDE + x) for z in ring for x in ring]
    else:
        pairs = [(z * SIDE + x, z * SIDE + (x + hop) % SIDE) for z in ring for x in ring]
    return lax.ppermute(value, "rep", pairs)


def place(axis):
    if axis == "y":
        return lax.axis_index("fs")
    rep = lax.axis_index("rep")
    return rep // SIDE if axis == "z" else rep % SIDE


def parts_for(value, extra, axis):
    me, dim, width = place(axis), DIMS[axis], value.shape[-1]
    sent = []
    for hop in HOPS:
        part = lax.dynamic_slice_in_dim(value, (me + hop) % SIDE, 1, dim).reshape(-1, width)
        sent.append(part if extra is None else jnp.concatenate([part, extra], axis=0))
    return sent, (lax.dynamic_slice_in_dim(value, me, 1, dim), extra)


def exchange(sent, axis):
    return [shift(part, axis, hop) for hop, part in zip(HOPS, sent)]


def four(own, one, three, two):
    return (own + two) + (one + three)


def two_parts(taps):
    high = lax.reduce_precision(taps, 8, 7)
    return high.astype(jnp.bfloat16), (taps - high).astype(jnp.bfloat16)


def add_up(kept, arrived):
    own, extra = kept
    width, count = own.shape[-1], own.size // own.shape[-1]
    heads = [own.reshape(count, width)] + [part[:count] for part in arrived]
    total = four(*[head.astype(jnp.float32) for head in heads])
    tails = None
    if extra is not None:
        tails = [extra] + [part[count:] for part in arrived]
    return total.astype(jnp.bfloat16).reshape(own.shape), tails


def gather_over(value, axis):
    one, three, two = exchange([value] * 3, axis)
    turn = (place(axis) + SIDE - jnp.arange(SIDE)) % SIDE
    turn = turn.reshape((SIDE,) + (1,) * value.ndim)
    return jnp.where(
        turn == 0, value, jnp.where(turn == 1, one, jnp.where(turn == 2, two, three))
    )


def backward_kernel(tp_ref, gate_ref, up_ref, cot_ref, tap_gate_ref, tap_up_ref, *rest):
    group_ref, stacked_ref, sums_ref, gate_pad, up_pad = rest[-5:]
    length = gate_ref.shape[0]
    zeros = jnp.zeros((HALO, LANES), jnp.float32)
    gate_pad[0:HALO, :] = zeros
    up_pad[0:HALO, :] = zeros
    gate_pad[HALO : HALO + length, :] = gate_ref[...].astype(jnp.float32)
    up_pad[HALO : HALO + length, :] = up_ref[...].astype(jnp.float32)
    kg = tap_gate_ref[...].astype(jnp.float32)
    ku = tap_up_ref[...].astype(jnp.float32)
    kg = [jnp.broadcast_to(kg[j : j + 1], (CHUNK, LANES)) for j in range(3)]
    ku = [jnp.broadcast_to(ku[j : j + 1], (CHUNK, LANES)) for j in range(3)]
    root = 0.7978845608028654
    count = length // CHUNK

    def delayed(pad, row):
        rows = pad[pl.ds(row, CHUNK + HALO), :]
        return [pltpu.roll(rows, 2, 0)[HALO:], pltpu.roll(rows, 1, 0)[HALO:], rows[HALO:]]

    def advanced(now, later, kernel):
        rows = jnp.concatenate([now, later], axis=0)
        one = pltpu.roll(rows, CHUNK + HALO - 1, 0)[:CHUNK]
        two = pltpu.roll(rows, CHUNK + HALO - 2, 0)[:CHUNK]
        return kernel[2] * now + kernel[1] * one + kernel[0] * two

    def folded(product):
        return jnp.sum(product.reshape(CHUNK // 8, 8, LANES), axis=0)

    def step(index, carry):
        later_gate, later_up, sums = carry
        row = pl.multiple_of((count - 1 - index) * CHUNK, CHUNK)
        gates = delayed(gate_pad, row)
        ups = delayed(up_pad, row)
        cot = cot_ref[pl.ds(row, CHUNK), :].astype(jnp.float32)
        v = kg[0] * gates[0] + kg[1] * gates[1] + kg[2] * gates[2]
        mixed_up = ku[0] * ups[0] + ku[1] * ups[1] + ku[2] * ups[2]
        square = v * v
        bent = jnp.tanh(v * (root + (root * 0.044715) * square))
        rise = 0.5 + 0.5 * bent
        slope = rise + (0.5 * v) * (1.0 - bent * bent) * (root + (3.0 * root * 0.044715) * square)
        back_gate = cot * mixed_up * slope
        back_up = cot * (v * rise)
        out_gate = advanced(back_gate, later_gate, kg).astype(jnp.bfloat16)
        out_up = advanced(back_up, later_up, ku).astype(jnp.bfloat16)
        for ref in (group_ref, stacked_ref):
            ref[pl.ds(row, CHUNK), 0:LANES] = out_gate
            ref[pl.ds(row, CHUNK), LANES : 2 * LANES] = out_up
        products = [back_gate * g for g in gates] + [back_up * u for u in ups]
        sums = tuple(s + folded(p) for s, p in zip(sums, products))
        return back_gate[:HALO], back_up[:HALO], sums

    start = (zeros, zeros, (zeros,) * 6)
    sums = lax.fori_loop(0, count, step, start)[2]
    rows = [jnp.sum(s, axis=0, keepdims=True) for s in sums]
    sums_ref[...] = jnp.concatenate(rows + [jnp.zeros((2, LANES), jnp.float32)], axis=0)


def backward(tp, pre_gate, pre_up, cotangent, taps_gate, taps_up, first, blocks, stacked):
    length, columns = pre_gate.shape
    total = columns // LANES
    wide = pl.BlockSpec((length, LANES), lambda j, t: (0, first + j))
    taps = pl.BlockSpec((3, LANES), lambda j, t: (0, t[0] * total + first + j))
    operands = [tp, pre_gate, pre_up, cotangent, taps_gate, taps_up]
    in_specs = [wide, wide, wide, taps, taps]
    aliases = {}
    if stacked is not None:
        aliases = {len(operands): 1}
        operands.append(stacked)
        in_specs.append(pl.BlockSpec(memory_space=pl.ANY))
    return pl.pallas_call(
        backward_kernel,
        grid_spec=pltpu.PrefetchScalarGridSpec(
            num_scalar_prefetch=1,
            grid=(blocks,),
            in_specs=in_specs,
            out_specs=[
                pl.BlockSpec((length, 2 * LANES), lambda j, t: (0, j)),
                pl.BlockSpec((length, 2 * LANES), lambda j, t: (0, first + j)),
                pl.BlockSpec((8, LANES), lambda j, t: (0, j)),
            ],
            scratch_shapes=[pltpu.VMEM((length + HALO, LANES), jnp.float32)] * 2,
        ),
        out_shape=[
            jax.ShapeDtypeStruct((length, blocks * 2 * LANES), jnp.bfloat16),
            jax.ShapeDtypeStruct((length, 2 * columns), jnp.bfloat16),
            jax.ShapeDtypeStruct((8, blocks * LANES), jnp.float32),
        ],
        input_output_aliases=aliases,
        cost_estimate=pl.CostEstimate(
            flops=2000 * length * LANES * blocks,
            bytes_accessed=length * LANES * blocks * 14,
            transcendentals=length * LANES * blocks,
        ),
        name="backward",
    )(*operands)


def weave_kernel(gate_ref, up_ref, out_ref):
    for block in range(gate_ref.shape[1] // LANES):
        columns = slice(block * LANES, (block + 1) * LANES)
        out_ref[:, 2 * block * LANES : (2 * block + 1) * LANES] = gate_ref[:, columns]
        out_ref[:, (2 * block + 1) * LANES : (2 * block + 2) * LANES] = up_ref[:, columns]


def weave(gate, up):
    rows, columns = gate.shape
    narrow = pl.BlockSpec((rows // SIDE, columns), lambda j: (j, 0))
    return pl.pallas_call(
        weave_kernel,
        grid=(SIDE,),
        in_specs=[narrow, narrow],
        out_specs=pl.BlockSpec((rows // SIDE, 2 * columns), lambda j: (j, 0)),
        out_shape=jax.ShapeDtypeStruct((rows, 2 * columns), gate.dtype),
        cost_estimate=pl.CostEstimate(
            flops=100 * rows * columns, bytes_accessed=8 * rows * columns, transcendentals=0
        ),
        name="weave",
    )(gate, up)


def join_kernel(place_ref, *refs):
    kept, got, out_ref, sums, sems = refs[:4], refs[4:8], refs[8], refs[9], refs[10]
    width = sums.shape[-1]
    copies = []
    for number, hop in enumerate((0,) + HOPS):
        total = kept[number][...].astype(jnp.float32) + got[number][...].astype(jnp.float32)
        sums[number] = total.astype(jnp.bfloat16)
        source = lax.rem(place_ref[0] + SIDE - hop, SIDE)
        target = out_ref.at[:, pl.ds(pl.multiple_of(source * width, width), width)]
        copies.append(pltpu.make_async_copy(sums.at[number], target, sems.at[number]))
        if number:
            copies[number - 1].start()
    copies[-1].start()
    for copy in copies:
        copy.wait()


def join(place_y, kept, got):
    rows, width = kept[0].shape
    return pl.pallas_call(
        join_kernel,
        in_specs=[pl.BlockSpec(memory_space=pltpu.SMEM)]
        + [pl.BlockSpec(memory_space=pltpu.VMEM)] * (2 * SIDE),
        out_specs=pl.BlockSpec(memory_space=pl.ANY),
        out_shape=jax.ShapeDtypeStruct((rows, SIDE * width), jnp.bfloat16),
        scratch_shapes=[
            pltpu.VMEM((SIDE, rows, width), jnp.bfloat16),
            pltpu.SemaphoreType.DMA((SIDE,)),
        ],
        cost_estimate=pl.CostEstimate(
            flops=400 * rows * width, bytes_accessed=24 * rows * width, transcendentals=0
        ),
        name="join",
    )(place_y, *kept, *got)


def finish_kernel(plan, factor, places, *refs):
    count = sum(len(lists) for _, _, lists in plan)
    pieces, outs = refs[:count], refs[count : count + 2]
    halves, sems = refs[count + 2 : -1], refs[-1]
    copies, number = [], 0

    def begin(index):
        for copy in copies[2 * index : 2 * index + 2]:
            copy.start()

    for low, axis, hops in plan:
        me = places[0] if axis == "z" else places[1]
        for hop in hops:
            piece, half = pieces[number], halves[number]
            width = piece.shape[-1] // 2
            for block in range(width // LANES):
                values = piece[:, :, 2 * block * LANES : 2 * (block + 1) * LANES]
                values = values.astype(jnp.float32) * factor
                half[0, :, :, block * LANES : (block + 1) * LANES] = values[:, :, :LANES]
                half[1, :, :, block * LANES : (block + 1) * LANES] = values[:, :, LANES:]
            source = lax.rem(me + SIDE - hop, SIDE)
            for side in range(2):
                columns = pl.ds(low * LANES, width)
                if axis == "z":
                    target = outs[side].at[source, :, :, columns]
                else:
                    target = outs[side].at[:, source, :, columns]
                copies.append(pltpu.make_async_copy(half.at[side], target, sems.at[number, side]))
            if number:
                begin(number - 1)
            number += 1
    begin(number - 1)
    for copy in copies:
        copy.wait()


def finish(places, plan, pieces, columns, factor):
    share = pieces[0].shape[1]
    out = jax.ShapeDtypeStruct((SIDE, SIDE, share, columns), jnp.float32)
    size = SIDE * SIDE * share * columns
    return pl.pallas_call(
        functools.partial(finish_kernel, plan, factor),
        in_specs=[pl.BlockSpec(memory_space=pltpu.SMEM)]
        + [pl.BlockSpec(memory_space=pltpu.VMEM)] * len(pieces),
        out_specs=[pl.BlockSpec(memory_space=pl.ANY)] * 2,
        out_shape=[out, out],
        scratch_shapes=[
            pltpu.VMEM((2, SIDE, share, p.shape[-1] // 2), jnp.float32) for p in pieces
        ]
        + [pltpu.SemaphoreType.DMA((len(pieces), 2))],
        cost_estimate=pl.CostEstimate(
            flops=200 * size, bytes_accessed=12 * size, transcendentals=0
        ),
        name="finish",
    )(places, *pieces)


def layer(inputs, pre_gate, pre_up, cotangent, w_gate, w_up, taps_gate, taps_up):
    columns = pre_gate.shape[2]
    reps, shards = lax.axis_size("rep"), lax.axis_size("fs")
    share = w_gate.shape[0] // reps
    tp = lax.axis_index("tp")
    swap = [(0, 1), (1, 0)]
    factor = float(pre_gate.shape[1] * reps * shards) ** (-0.5)

    shard = weave(w_gate, w_up)
    below, above = shift(shard, "y", 1), shift(shard, "y", SIDE - 1)
    middle_row = shard.shape[0] // 2
    opposite = [shift(below[:middle_row], "y", 1), shift(above[middle_row:], "y", SIDE - 1)]

    half = inputs.shape[1]
    own_rows = inputs[0]
    other_rows = lax.ppermute(own_rows, "tp", swap)
    first = jnp.where(tp == 0, own_rows, other_rows)
    second = jnp.where(tp == 0, other_rows, own_rows)
    whole_rows = jnp.concatenate([first, second], axis=0)

    where = jnp.full((1,), tp, jnp.int32)
    stacked, low, groups, tap_sums = None, 0, [], []
    for blocks, _ in GROUPS:
        group, stacked, taps = backward(
            where, pre_gate[0], pre_up[0], cotangent[0], taps_gate, taps_up, low, blocks, stacked
        )
        low += blocks
        groups.append(group)
        tap_sums.append(taps)
    taps = jnp.concatenate(tap_sums, axis=1)
    wide = groups[0].shape[1]
    taps = jnp.pad(taps, ((0, 0), (0, wide - columns)))
    extra = jnp.concatenate(two_parts(taps), axis=0)

    begun = []
    for group, (_, order) in zip(groups, GROUPS):
        value = jnp.einsum("nd,nk->dk", whole_rows, group, preferred_element_type=jnp.float32)
        value = value.astype(jnp.bfloat16).reshape(SIDE, SIDE, SIDE, share, group.shape[1])
        sent, kept = parts_for(value, extra, order[0])
        extra = None
        begun.append((kept, exchange(sent, order[0])))

    lower = lax.optimization_barrier(lax.optimization_barrier(tp) == 0)
    upper = lax.optimization_barrier(lax.optimization_barrier(tp) == 1)

    def folded(tails):
        return four(*[t[:8].astype(jnp.float32) + t[8:].astype(jnp.float32) for t in tails])

    middle = []
    for (kept, arrived), (_, order) in zip(begun, GROUPS):
        value, tails = add_up(kept, arrived)
        extra = None if tails is None else jnp.concatenate(two_parts(folded(tails)), axis=0)
        sent, kept = parts_for(value, extra, order[1])
        middle.append((kept, exchange(sent, order[1])))

    values = []
    for kept, arrived in middle:
        value, tails = add_up(kept, arrived)
        values.append(value.reshape(SIDE, 1, 1, share, value.shape[-1]))
        if tails is not None:
            taps = folded(tails)[:, :columns]
    both = jnp.concatenate(values, axis=-1)
    sent, kept = parts_for(both, jnp.concatenate(two_parts(taps), axis=1), "y")
    arrived = exchange(sent, "y")
    value, tails = add_up(kept, arrived)
    value = value.reshape(share, 2 * columns)
    taps = four(
        *[t[:, :columns].astype(jnp.float32) + t[:, columns:].astype(jnp.float32) for t in tails]
    )

    low, plan, pieces, parts = 0, [], [], []
    for blocks, order in GROUPS:
        part = value[:, 2 * LANES * low : 2 * LANES * (low + blocks)]
        parts.append(gather_over(part, order[0]))
        plan.append((low, order[1], (0,) + HOPS))
        low += blocks
    for part, (_, order) in zip(parts, GROUPS):
        pieces += [part] + exchange([part] * 3, order[1])
    places = jnp.stack([place("z"), place("x")]).astype(jnp.int32)
    grads = finish(places, tuple(plan), pieces, columns, factor)
    grads = [g.reshape(reps * share, columns) for g in grads]

    taps = taps * factor
    other_taps = lax.ppermute(taps, "tp", swap)
    grad_taps = [
        jnp.concatenate([jnp.where(ours, t, o), jnp.where(ours, o, t)], axis=1)
        for ours, t, o in (
            (lower, taps[:3], other_taps[:3]),
            (jnp.logical_not(upper), taps[3:6], other_taps[3:6]),
        )
    ]

    def project(w):
        result = jnp.einsum("nk,dk->nd", stacked, w, preferred_element_type=jnp.float32)
        return result.astype(jnp.bfloat16)

    partials = [project(shard), project(below), project(above)]
    partials.append(jnp.concatenate([project(w) for w in opposite], axis=1))
    away = [lax.dynamic_slice_in_dim(p, (1 - tp) * half, half, 0) for p in partials]
    kept = [lax.dynamic_slice_in_dim(p, tp * half, half, 0) for p in partials]
    got = [lax.ppermute(p, "tp", swap) for p in away]
    grad_inputs = join(jnp.full((1,), place("y"), jnp.int32), kept, got)[None]
    return (grad_inputs, grads[0], grads[1], grad_taps[0], grad_taps[1])


def solution(mesh):
    placed = (
        P(("rep", "fs"), "tp", None),
        P(("rep", "fs"), None, "tp"),
        P(("rep", "fs"), None, "tp"),
        P(("rep", "fs"), None, "tp"),
        P("fs", "tp"),
        P("fs", "tp"),
        P(),
        P(),
    )
    return jax.shard_map(
        layer,
        mesh=mesh,
        in_specs=placed,
        out_specs=(P(("rep", "fs"), "tp", None), P("fs", "tp"), P("fs", "tp"), P(), P()),
        check_vma=False,
    )
```

profile of v0, /device:TPU:1, one launch (start us, length us, event | category | flops | bytes accessed | tf_op | source)
XLA Modules:
  0.0 230.2 jit_solution(453450731093523353)
XLA Ops:
  0.6 4.2 %weave.1 = bf16[512,2816]{1,0:T(8,128)(2,1)} custom-call(bf16[512,1408]{1,0:T(8,128)(2,1)} %gate_ref.1, bf16[512,1408]{1,0:T(8,128)(2,1)} %up_ref.1), custom_call_target="tpu_custom_call" | custom-call | flops 72089600 | bytes 5767168 | tf_op jit(solution)/shard_map/weave/pallas_call | solution.py:187
  9.5 9.7 %backward.2 = (bf16[768,1536]{1,0:T(8,128)(2,1)}, bf16[768,2816]{1,0:T(8,128)(2,1)}, f32[8,768]{1,0:T(8,128)}) custom-call(s32[1]{0:T(128)} %bitcast.1.tp_ref, bf16[768,1408]{1,0:T(8,128)(2,1)} %bitcast.82, bf16[768,1408]{1,0:T(8,128)(2,1)} %bitcast.84, bf16[768,1408]{1,0:T(8,128)(2,1)} %bitcast.86, bf16[3,2816]{1,0:T(4,128)(2,1)} %tap_gate_ref.3, ...), custom_call_target="tpu_custom_call" | custom-call | flops 1179648000 | bytes 8257536 | tf_op jit(solution)/shard_map/backward/pallas_call | solution.py:149
  19.2 8.7 %backward.3 = (bf16[768,1280]{1,0:T(8,128)(2,1)}, bf16[768,2816]{1,0:T(8,128)(2,1)}, f32[8,640]{1,0:T(8,128)}) custom-call(s32[1]{0:T(128)} %bitcast.1.tp_ref, bf16[768,1408]{1,0:T(8,128)(2,1)} %bitcast.83, bf16[768,1408]{1,0:T(8,128)(2,1)} %bitcast.85, bf16[768,1408]{1,0:T(8,128)(2,1)} %bitcast.87, ...), custom_call_target="tpu_custom_call", output_to_operand_aliasing={{1}: (6, {})} | custom-call | flops 983040000 | bytes 6881280 | tf_op jit(solution)/shard_map/backward/pallas_call | solution.py:149
  28.6 4.7 %convolution_convert_fusion.4 = bf16[768,512]{1,0:T(8,128)(2,1)S(1)} fusion(bf16[768,2816]{1,0:T(8,128)(2,1)} %get-tuple-element.14, bf16[512,2816]{1,0:T(8,128)(2,1)S(1)} %copy-done), kind=kOutput, calls=%fused_computation.19 | convolution fusion | flops 2214985728 | bytes 7995392 | tf_op jit(solution)/shard_map/nk,dk->nd/dot_general | solution.py:386
  36.7 4.7 %convolution_convert_fusion.1 = bf16[2048,1280]{1,0:T(8,128)(2,1)S(1)} fusion(bf16[768,1280]{1,0:T(8,128)(2,1)S(1)} %copy-done.16, bf16[384,2048]{1,0:T(8,128)(2,1)S(1)} %get-tuple-element.34, bf16[384,2048]{1,0:T(8,128)(2,1)S(1)} %get-tuple-element.33), kind=kOutput, calls=%fused_computation.1 | convolution fusion | flops 4035444736 | bytes 10354688 | tf_op jit(solution)/shard_map/nd,nk->dk/dot_general | solution.py:329
  44.6 5.4 %convolution_convert_fusion = bf16[2048,1536]{1,0:T(8,128)(2,1)S(1)} fusion(bf16[768,1536]{1,0:T(8,128)(2,1)S(1)} %copy-done.15, bf16[384,2048]{1,0:T(8,128)(2,1)S(1)} %get-tuple-element.34, bf16[384,2048]{1,0:T(8,128)(2,1)S(1)} %get-tuple-element.33), kind=kOutput, calls=%fused_computation | convolution fusion | flops 4841275392 | bytes 11796480 | tf_op jit(solution)/shard_map/nd,nk->dk/dot_general | solution.py:329
  51.2 3.8 %collective-permute-start.11 = (bf16[528,1536]{1,0:T(8,128)(2,1)S(1)}, bf16[528,1536]{1,0:T(8,128)(2,1)S(1)}, u32[]{:S(2)}, u32[]{:S(2)}) collective-permute-start(bf16[528,1536]{1,0:T(8,128)(2,1)S(1)} %get-tuple-element.69), channel_id=1, source_target_pairs={{0,96},{8,104},{16,112},{24,120},{32,0},{40,8},{48,16},{56,24},{64... | collective-permute-start | bytes 4866056 | tf_op jit(solution)/shard_map/ppermute | solution.py:28
  55.0 15.8 %collective-permute-done = bf16[512,2816]{1,0:T(8,128)(2,1)} collective-permute-done((bf16[512,2816]{1,0:T(8,128)(2,1)}, bf16[512,2816]{1,0:T(8,128)(2,1)}, u32[]{:S(2)}, u32[]{:S(2)}) %collective-permute-start) | collective-permute-done | bytes 2883616 | tf_op jit(solution)/shard_map/ppermute | solution.py:23
  77.6 4.2 %convolution_convert_fusion.3 = bf16[768,512]{1,0:T(8,128)(2,1)S(1)} fusion(bf16[768,2816]{1,0:T(8,128)(2,1)S(1)} %bitcast.96, bf16[512,2816]{1,0:T(8,128)(2,1)} %collective-permute-done), kind=kOutput, calls=%fused_computation.18 | convolution fusion | flops 2214985728 | bytes 7995392 | tf_op jit(solution)/shard_map/nk,dk->nd/dot_general | solution.py:386
  81.8 3.7 %collective-permute-start.9 = (bf16[528,1536]{1,0:T(8,128)(2,1)S(1)}, bf16[528,1536]{1,0:T(8,128)(2,1)S(1)}, u32[]{:S(2)}, u32[]{:S(2)}) collective-permute-start(bf16[528,1536]{1,0:T(8,128)(2,1)S(1)} %get-tuple-element.67), channel_id=1, source_target_pairs={{0,64},{8,72},{16,80},{24,88},{32,96},{40,104},{48,112},{56,120},{... | collective-permute-start | bytes 4866056 | tf_op jit(solution)/shard_map/ppermute | solution.py:28
  85.5 4.2 %convolution_convert_fusion.2 = bf16[768,512]{1,0:T(8,128)(2,1)S(1)} fusion(bf16[768,2816]{1,0:T(8,128)(2,1)S(1)} %bitcast.96, bf16[512,2816]{1,0:T(8,128)(2,1)} %collective-permute-done.1), kind=kOutput, calls=%fused_computation.17 | convolution fusion | flops 2214985728 | bytes 7995392 | tf_op jit(solution)/shard_map/nk,dk->nd/dot_general | solution.py:386
  89.7 11.2 %collective-permute-done.16 = bf16[512,1280]{1,0:T(8,128)(2,1)S(1)} collective-permute-done((bf16[512,1280]{1,0:T(8,128)(2,1)S(1)}, bf16[512,1280]{1,0:T(8,128)(2,1)S(1)}, u32[]{:S(2)}, u32[]{:S(2)}) %collective-permute-start.16) | collective-permute-done | bytes 1310752 | tf_op jit(solution)/shard_map/ppermute | solution.py:28
  101.0 28.9 %collective-permute-done.15 = bf16[512,1280]{1,0:T(8,128)(2,1)S(1)} collective-permute-done((bf16[512,1280]{1,0:T(8,128)(2,1)S(1)}, bf16[512,1280]{1,0:T(8,128)(2,1)S(1)}, u32[]{:S(2)}, u32[]{:S(2)}) %collective-permute-start.15) | collective-permute-done | bytes 1310752 | tf_op jit(solution)/shard_map/ppermute | solution.py:28
  132.1 3.8 %collective-permute-start.20 = (bf16[128,1280]{1,0:T(8,128)(2,1)S(1)}, bf16[128,1280]{1,0:T(8,128)(2,1)S(1)}, u32[]{:S(2)}, u32[]{:S(2)}) collective-permute-start(bf16[128,1280]{1,0:T(8,128)(2,1)S(1)} %bitcast.110), channel_id=1, source_target_pairs={{0,96},{8,104},{16,112},{24,120},{32,0},{40,8},{48,16},{56,24},{64... | collective-permute-start | bytes 983048 | tf_op jit(solution)/shard_map/ppermute | solution.py:28
  142.1 3.9 %collective-permute-done.19 = bf16[128,1280]{1,0:T(8,128)(2,1)S(1)} collective-permute-done((bf16[128,1280]{1,0:T(8,128)(2,1)S(1)}, bf16[128,1280]{1,0:T(8,128)(2,1)S(1)}, u32[]{:S(2)}, u32[]{:S(2)}) %collective-permute-start.19) | collective-permute-done | bytes 327712 | tf_op jit(solution)/shard_map/ppermute | solution.py:28
  149.9 9.1 %collective-permute-done.13 = bf16[144,1536]{1,0:T(8,128)(2,1)S(1)} collective-permute-done((bf16[144,1536]{1,0:T(8,128)(2,1)S(1)}, bf16[144,1536]{1,0:T(8,128)(2,1)S(1)}, u32[]{:S(2)}, u32[]{:S(2)}) %collective-permute-start.13) | collective-permute-done | bytes 442400 | tf_op jit(solution)/shard_map/ppermute | solution.py:28
  165.8 3.2 %collective-permute-done.22 = bf16[40,2816]{1,0:T(8,128)(2,1)S(1)} collective-permute-done((bf16[40,2816]{1,0:T(8,128)(2,1)S(1)}, bf16[40,2816]{1,0:T(8,128)(2,1)S(1)}, u32[]{:S(2)}, u32[]{:S(2)}) %collective-permute-start.22) | collective-permute-done | bytes 225312 | tf_op jit(solution)/shard_map/ppermute | solution.py:23
  174.6 5.4 %collective-permute-start.25 = (bf16[32,1536]{1,0:T(8,128)(2,1)S(1)}, bf16[32,1536]{1,0:T(8,128)(2,1)S(1)}, u32[]{:S(2)}, u32[]{:S(2)}) collective-permute-start(bf16[32,1536]{1,0:T(8,128)(2,1)S(1)} %slice.202), channel_id=1, source_target_pairs={{0,64},{8,72},{16,80},{24,88},{32,96},{40,104},{48,112},{56,120},{... | collective-permute-start | bytes 294920 | tf_op jit(solution)/shard_map/ppermute | solution.py:28
  180.1 9.2 %collective-permute-start.36 = (f32[8,1408]{1,0:T(8,128)S(1)}, f32[8,1408]{1,0:T(8,128)S(1)}, u32[]{:S(2)}, u32[]{:S(2)}) collective-permute-start(f32[8,1408]{1,0:T(8,128)S(1)} %add_multiply_fusion), channel_id=1, source_target_pairs={{0,1},{1,0},{2,3},{3,2},{4,5},{5,4},{6,7},{7,6},{8,9},{9,8},{10,11... | collective-permute-start | bytes 135176 | tf_op jit(solution)/shard_map/ppermute | solution.py:376
  199.2 3.8 %collective-permute-start.4 = (bf16[384,512]{1,0:T(8,128)(2,1)}, bf16[384,512]{1,0:T(8,128)(2,1)S(1)}, u32[]{:S(2)}, u32[]{:S(2)}) collective-permute-start(bf16[384,512]{1,0:T(8,128)(2,1)} %get-tuple-element.49), channel_id=1, source_target_pairs={{0,1},{1,0},{2,3},{3,2},{4,5},{5,4},{6,7},{7,6},{8,9},{9,8},{10,11... | collective-permute-start | bytes 1179656 | tf_op jit(solution)/shard_map/ppermute | solution.py:393
  202.9 4.1 %collective-permute-start.5 = (bf16[384,512]{1,0:T(8,128)(2,1)}, bf16[384,512]{1,0:T(8,128)(2,1)S(1)}, u32[]{:S(2)}, u32[]{:S(2)}) collective-permute-start(bf16[384,512]{1,0:T(8,128)(2,1)} %get-tuple-element.47), channel_id=1, source_target_pairs={{0,1},{1,0},{2,3},{3,2},{4,5},{5,4},{6,7},{7,6},{8,9},{9,8},{10,11... | collective-permute-start | bytes 1179656 | tf_op jit(solution)/shard_map/ppermute | solution.py:393
  210.9 9.6 %collective-permute-done.29.refs_3_ = bf16[4,32,1536]{2,1,0:T(8,128)(2,1)S(1)} collective-permute-done((bf16[4,32,1536]{2,1,0:T(8,128)(2,1)S(1)}, bf16[4,32,1536]{2,1,0:T(8,128)(2,1)S(1)}, u32[]{:S(2)}, u32[]{:S(2)}) %collective-permute-start.29) | collective-permute-done | bytes 393248 | tf_op jit(solution)/shard_map/ppermute | solution.py:28
  221.2 4.5 %finish.1 = (f32[4,4,32,1408]{3,2,1,0:T(8,128)}, f32[4,4,32,1408]{3,2,1,0:T(8,128)}) custom-call(s32[2]{0:T(128)} %pad_add_fusion.places, bf16[4,32,1536]{2,1,0:T(8,128)(2,1)} %copy-done.1, bf16[4,32,1536]{2,1,0:T(8,128)(2,1)} %copy-done.4, bf16[4,32,1536]{2,1,0:T(8,128)(2,1)} %copy-done.6, bf16[4,32,1536]{2,1,0:T(8,128)(2,1)} %copy-done.9, ...), custom_call_target="tpu_custom_call" | custom-call | flops 144179200 | bytes 8650752 | tf_op jit(solution)/shard_map/finish/pallas_call | solution.py:276
  226.9 3.2 %join.1 = bf16[384,2048]{1,0:T(8,128)(2,1)} custom-call(s32[1]{0:T(128)} %bitcast.place_ref, bf16[384,512]{1,0:T(8,128)(2,1)} %get-tuple-element.50.refs_0_, bf16[384,512]{1,0:T(8,128)(2,1)} %get-tuple-element.48.refs_1_, bf16[384,512]{1,0:T(8,128)(2,1)} %get-tuple-element.46.refs_2_, bf16[384,512]{1,0:T(8,128)(2,1)} %get-tuple-element.44.refs_3_, ...), custom_call_target="tpu_custom_call" | custom-call | flops 78643200 | bytes 4718592 | tf_op jit(solution)/shard_map/join/pallas_call | solution.py:219
  (141 shorter events, 60.0 us)
Async XLA Ops:
  4.8 65.9 %collective-permute-start = (bf16[512,2816]{1,0:T(8,128)(2,1)}, bf16[512,2816]{1,0:T(8,128)(2,1)}, u32[]{:S(2)}, u32[]{:S(2)}) collective-permute-start(bf16[512,2816]{1,0:T(8,128)(2,1)} %weave.1), channel_id=1, source_target_pairs={{0,2},{2,4},{4,6},{6,0},{1,3},{3,5},{5,7},{7,1},{8,10},{10,12},{12... | collective-permute-start | bytes 8650760 | tf_op jit(solution)/shard_map/ppermute | solution.py:23
  7.0 66.4 %collective-permute-start.1 = (bf16[512,2816]{1,0:T(8,128)(2,1)}, bf16[512,2816]{1,0:T(8,128)(2,1)}, u32[]{:S(2)}, u32[]{:S(2)}) collective-permute-start(bf16[512,2816]{1,0:T(8,128)(2,1)} %weave.1), channel_id=1, source_target_pairs={{0,6},{2,0},{4,2},{6,4},{1,7},{3,1},{5,3},{7,5},{8,14},{10,8},{12,... | collective-permute-start | bytes 8650760 | tf_op jit(solution)/shard_map/ppermute | solution.py:23
  8.4 25.9 %collective-permute-start.8 = (bf16[384,2048]{1,0:T(8,128)(2,1)}, bf16[384,2048]{1,0:T(8,128)(2,1)}, u32[]{:S(2)}, u32[]{:S(2)}) collective-permute-start(bf16[384,2048]{1,0:T(8,128)(2,1)} %bitcast.8), channel_id=1, source_target_pairs={{0,1},{1,0},{2,3},{3,2},{4,5},{5,4},{6,7},{7,6},{8,9},{9,8},{10,11... | collective-permute-start | bytes 4718600 | tf_op jit(solution)/shard_map/ppermute | solution.py:308
  41.9 39.9 %collective-permute-start.17 = (bf16[512,1280]{1,0:T(8,128)(2,1)S(1)}, bf16[512,1280]{1,0:T(8,128)(2,1)S(1)}, u32[]{:S(2)}, u32[]{:S(2)}) collective-permute-start(bf16[512,1280]{1,0:T(8,128)(2,1)S(1)} %bitcast.107), channel_id=1, source_target_pairs={{0,24},{8,0},{16,8},{24,16},{32,56},{40,32},{48,40},{56,48},{64,88... | collective-permute-start | bytes 3932168 | tf_op jit(solution)/shard_map/ppermute | solution.py:28
  51.2 80.9 %collective-permute-start.11 = (bf16[528,1536]{1,0:T(8,128)(2,1)S(1)}, bf16[528,1536]{1,0:T(8,128)(2,1)S(1)}, u32[]{:S(2)}, u32[]{:S(2)}) collective-permute-start(bf16[528,1536]{1,0:T(8,128)(2,1)S(1)} %get-tuple-element.69), channel_id=1, source_target_pairs={{0,96},{8,104},{16,112},{24,120},{32,0},{40,8},{48,16},{56,24},{64... | collective-permute-start | bytes 4866056 | tf_op jit(solution)/shard_map/ppermute | solution.py:28
  55.0 80.9 %collective-permute-start.10 = (bf16[528,1536]{1,0:T(8,128)(2,1)S(1)}, bf16[528,1536]{1,0:T(8,128)(2,1)S(1)}, u32[]{:S(2)}, u32[]{:S(2)}) collective-permute-start(bf16[528,1536]{1,0:T(8,128)(2,1)S(1)} %get-tuple-element.68), channel_id=1, source_target_pairs={{0,32},{8,40},{16,48},{24,56},{32,64},{40,72},{48,80},{56,88},{64,... | collective-permute-start | bytes 4866056 | tf_op jit(solution)/shard_map/ppermute | solution.py:28
  70.8 30.2 %collective-permute-start.16 = (bf16[512,1280]{1,0:T(8,128)(2,1)S(1)}, bf16[512,1280]{1,0:T(8,128)(2,1)S(1)}, u32[]{:S(2)}, u32[]{:S(2)}) collective-permute-start(bf16[512,1280]{1,0:T(8,128)(2,1)S(1)} %bitcast.106), channel_id=1, source_target_pairs={{0,8},{8,16},{16,24},{24,0},{32,40},{40,48},{48,56},{56,32},{64,72... | collective-permute-start | bytes 3932168 | tf_op jit(solution)/shard_map/ppermute | solution.py:28
  73.4 56.5 %collective-permute-start.15 = (bf16[512,1280]{1,0:T(8,128)(2,1)S(1)}, bf16[512,1280]{1,0:T(8,128)(2,1)S(1)}, u32[]{:S(2)}, u32[]{:S(2)}) collective-permute-start(bf16[512,1280]{1,0:T(8,128)(2,1)S(1)} %bitcast.105), channel_id=1, source_target_pairs={{0,16},{8,24},{16,0},{24,8},{32,48},{40,56},{48,32},{56,40},{64,80... | collective-permute-start | bytes 3932168 | tf_op jit(solution)/shard_map/ppermute | solution.py:28
  81.8 54.1 %collective-permute-start.9 = (bf16[528,1536]{1,0:T(8,128)(2,1)S(1)}, bf16[528,1536]{1,0:T(8,128)(2,1)S(1)}, u32[]{:S(2)}, u32[]{:S(2)}) collective-permute-start(bf16[528,1536]{1,0:T(8,128)(2,1)S(1)} %get-tuple-element.67), channel_id=1, source_target_pairs={{0,64},{8,72},{16,80},{24,88},{32,96},{40,104},{48,112},{56,120},{... | collective-permute-start | bytes 4866056 | tf_op jit(solution)/shard_map/ppermute | solution.py:28
  101.0 91.2 %collective-permute-start.2 = (bf16[256,2816]{1,0:T(8,128)(2,1)S(1)}, bf16[256,2816]{1,0:T(8,128)(2,1)S(1)}, u32[]{:S(2)}, u32[]{:S(2)}) collective-permute-start(bf16[256,2816]{1,0:T(8,128)(2,1)S(1)} %slice.171), channel_id=1, source_target_pairs={{0,2},{2,4},{4,6},{6,0},{1,3},{3,5},{5,7},{7,1},{8,10},{10,12},{12... | collective-permute-start | bytes 4325384 | tf_op jit(solution)/shard_map/ppermute | solution.py:23
  129.8 65.4 %collective-permute-start.3 = (bf16[256,2816]{1,0:T(8,128)(2,1)S(1)}, bf16[256,2816]{1,0:T(8,128)(2,1)S(1)}, u32[]{:S(2)}, u32[]{:S(2)}) collective-permute-start(bf16[256,2816]{1,0:T(8,128)(2,1)S(1)} %slice.172), channel_id=1, source_target_pairs={{0,6},{2,0},{4,2},{6,4},{1,7},{3,1},{5,3},{7,5},{8,14},{10,8},{12,... | collective-permute-start | bytes 4325384 | tf_op jit(solution)/shard_map/ppermute | solution.py:23
  135.9 13.2 %collective-permute-start.18 = (bf16[128,1280]{1,0:T(8,128)(2,1)S(1)}, bf16[128,1280]{1,0:T(8,128)(2,1)S(1)}, u32[]{:S(2)}, u32[]{:S(2)}) collective-permute-start(bf16[128,1280]{1,0:T(8,128)(2,1)S(1)} %bitcast.108), channel_id=1, source_target_pairs={{0,64},{8,72},{16,80},{24,88},{32,96},{40,104},{48,112},{56,120},{... | collective-permute-start | bytes 983048 | tf_op jit(solution)/shard_map/ppermute | solution.py:28
  146.0 12.9 %collective-permute-start.13 = (bf16[144,1536]{1,0:T(8,128)(2,1)S(1)}, bf16[144,1536]{1,0:T(8,128)(2,1)S(1)}, u32[]{:S(2)}, u32[]{:S(2)}) collective-permute-start(bf16[144,1536]{1,0:T(8,128)(2,1)S(1)} %get-tuple-element.65), channel_id=1, source_target_pairs={{0,8},{8,16},{16,24},{24,0},{32,40},{40,48},{48,56},{56,32},{64,72... | collective-permute-start | bytes 1327112 | tf_op jit(solution)/shard_map/ppermute | solution.py:28
  174.6 14.8 %collective-permute-start.25 = (bf16[32,1536]{1,0:T(8,128)(2,1)S(1)}, bf16[32,1536]{1,0:T(8,128)(2,1)S(1)}, u32[]{:S(2)}, u32[]{:S(2)}) collective-permute-start(bf16[32,1536]{1,0:T(8,128)(2,1)S(1)} %slice.202), channel_id=1, source_target_pairs={{0,64},{8,72},{16,80},{24,88},{32,96},{40,104},{48,112},{56,120},{... | collective-permute-start | bytes 294920 | tf_op jit(solution)/shard_map/ppermute | solution.py:28
  180.1 14.0 %collective-permute-start.36 = (f32[8,1408]{1,0:T(8,128)S(1)}, f32[8,1408]{1,0:T(8,128)S(1)}, u32[]{:S(2)}, u32[]{:S(2)}) collective-permute-start(f32[8,1408]{1,0:T(8,128)S(1)} %add_multiply_fusion), channel_id=1, source_target_pairs={{0,1},{1,0},{2,3},{3,2},{4,5},{5,4},{6,7},{7,6},{8,9},{9,8},{10,11... | collective-permute-start | bytes 135176 | tf_op jit(solution)/shard_map/ppermute | solution.py:376
  190.0 12.9 %collective-permute-start.34 = (bf16[4,32,1280]{2,1,0:T(8,128)(2,1)S(1)}, bf16[4,32,1280]{2,1,0:T(8,128)(2,1)S(1)}, u32[]{:S(2)}, u32[]{:S(2)}) collective-permute-start(bf16[4,32,1280]{2,1,0:T(8,128)(2,1)S(1)} %select_select_fusion.1.refs_4_), channel_id=1, source_target_pairs={{0,96},{8,104},{16,112},{24,120},{32,0},{40,8},{48,16},{56,24},{64... | collective-permute-start | bytes 983048 | tf_op jit(solution)/shard_map/ppermute | solution.py:28
  192.2 14.8 %collective-permute-start.35 = (bf16[4,32,1280]{2,1,0:T(8,128)(2,1)S(1)}, bf16[4,32,1280]{2,1,0:T(8,128)(2,1)S(1)}, u32[]{:S(2)}, u32[]{:S(2)}) collective-permute-start(bf16[4,32,1280]{2,1,0:T(8,128)(2,1)S(1)} %select_select_fusion.1.refs_4_), channel_id=1, source_target_pairs={{0,64},{8,72},{16,80},{24,88},{32,96},{40,104},{48,112},{56,120},{... | collective-permute-start | bytes 983048 | tf_op jit(solution)/shard_map/ppermute | solution.py:28
  194.1 14.1 %collective-permute-start.27 = (bf16[4,32,1536]{2,1,0:T(8,128)(2,1)S(1)}, bf16[4,32,1536]{2,1,0:T(8,128)(2,1)S(1)}, u32[]{:S(2)}, u32[]{:S(2)}) collective-permute-start(bf16[4,32,1536]{2,1,0:T(8,128)(2,1)S(1)} %select_select_fusion.refs_0_), channel_id=1, source_target_pairs={{0,8},{8,16},{16,24},{24,0},{32,40},{40,48},{48,56},{56,32},{64,72... | collective-permute-start | bytes 1179656 | tf_op jit(solution)/shard_map/ppermute | solution.py:28
  195.2 14.7 %collective-permute-start.28 = (bf16[4,32,1536]{2,1,0:T(8,128)(2,1)S(1)}, bf16[4,32,1536]{2,1,0:T(8,128)(2,1)S(1)}, u32[]{:S(2)}, u32[]{:S(2)}) collective-permute-start(bf16[4,32,1536]{2,1,0:T(8,128)(2,1)S(1)} %select_select_fusion.refs_0_), channel_id=1, source_target_pairs={{0,24},{8,0},{16,8},{24,16},{32,56},{40,32},{48,40},{56,48},{64,88... | collective-permute-start | bytes 1179656 | tf_op jit(solution)/shard_map/ppermute | solution.py:28
  199.2 26.5 %collective-permute-start.4 = (bf16[384,512]{1,0:T(8,128)(2,1)}, bf16[384,512]{1,0:T(8,128)(2,1)S(1)}, u32[]{:S(2)}, u32[]{:S(2)}) collective-permute-start(bf16[384,512]{1,0:T(8,128)(2,1)} %get-tuple-element.49), channel_id=1, source_target_pairs={{0,1},{1,0},{2,3},{3,2},{4,5},{5,4},{6,7},{7,6},{8,9},{9,8},{10,11... | collective-permute-start | bytes 1179656 | tf_op jit(solution)/shard_map/ppermute | solution.py:393
  202.9 22.8 %collective-permute-start.5 = (bf16[384,512]{1,0:T(8,128)(2,1)}, bf16[384,512]{1,0:T(8,128)(2,1)S(1)}, u32[]{:S(2)}, u32[]{:S(2)}) collective-permute-start(bf16[384,512]{1,0:T(8,128)(2,1)} %get-tuple-element.47), channel_id=1, source_target_pairs={{0,1},{1,0},{2,3},{3,2},{4,5},{5,4},{6,7},{7,6},{8,9},{9,8},{10,11... | collective-permute-start | bytes 1179656 | tf_op jit(solution)/shard_map/ppermute | solution.py:393
  207.0 18.7 %collective-permute-start.6 = (bf16[384,512]{1,0:T(8,128)(2,1)}, bf16[384,512]{1,0:T(8,128)(2,1)S(1)}, u32[]{:S(2)}, u32[]{:S(2)}) collective-permute-start(bf16[384,512]{1,0:T(8,128)(2,1)} %get-tuple-element.45), channel_id=1, source_target_pairs={{0,1},{1,0},{2,3},{3,2},{4,5},{5,4},{6,7},{7,6},{8,9},{9,8},{10,11... | collective-permute-start | bytes 1179656 | tf_op jit(solution)/shard_map/ppermute | solution.py:393
  208.2 12.2 %collective-permute-start.29 = (bf16[4,32,1536]{2,1,0:T(8,128)(2,1)S(1)}, bf16[4,32,1536]{2,1,0:T(8,128)(2,1)S(1)}, u32[]{:S(2)}, u32[]{:S(2)}) collective-permute-start(bf16[4,32,1536]{2,1,0:T(8,128)(2,1)S(1)} %select_select_fusion.refs_0_), channel_id=1, source_target_pairs={{0,16},{8,24},{16,0},{24,8},{32,48},{40,56},{48,32},{56,40},{64,80... | collective-permute-start | bytes 1179656 | tf_op jit(solution)/shard_map/ppermute | solution.py:28
  209.9 15.9 %collective-permute-start.7 = (bf16[384,512]{1,0:T(8,128)(2,1)}, bf16[384,512]{1,0:T(8,128)(2,1)S(1)}, u32[]{:S(2)}, u32[]{:S(2)}) collective-permute-start(bf16[384,512]{1,0:T(8,128)(2,1)} %get-tuple-element.43), channel_id=1, source_target_pairs={{0,1},{1,0},{2,3},{3,2},{4,5},{5,4},{6,7},{7,6},{8,9},{9,8},{10,11... | collective-permute-start | bytes 1179656 | tf_op jit(solution)/shard_map/ppermute | solution.py:393
  (32 other events, 266.4 us)
where the time goes:
time: 231 us; the launch traced here: 230 us
  waiting for transfers between devices  91.1 us (39%)
  starting transfers between devices  64.5 us (28%)
  Pallas kernels  30.2 us (13%)
  matrix products  25.8 us (11%)
  local copies, waits for them, and re-layouts  9.4 us (4%)
  other arithmetic  7.82 us (3%)
    ppermute x24, waiting for transfers between devices, shift(): return lax.ppermute(value, 'rep', pairs)  70.3 us
    ppermute x24, starting transfers between devices, shift(): return lax.ppermute(value, 'rep', pairs)  37.9 us
    ppermute x7, waiting for transfers between devices, shift(): return lax.ppermute(value, 'fs', [(i, (i + hop) % SIDE) for i in ring])  20.8 us
    pallas_call x2, Pallas kernels, backward(): pl.pallas_call(backward_kernel, grid_spec=pltpu.PrefetchScalarGridSpec(nu...  18.3 us
    dot_general x5, matrix products, project(): jnp.einsum('nk,dk->nd', stacked, w, preferred_element_type=jnp.float32)  15.7 us
    dot_general x2, matrix products, layer(): jnp.einsum('nd,nk->dk', whole_rows, group, preferred_element_type=jnp.flo...  10.1 us
    ppermute x4, starting transfers between devices, layer(): got = [lax.ppermute(p, 'tp', swap) for p in away]  9.34 us
    ppermute x1, starting transfers between devices, layer(): other_taps = lax.ppermute(taps, 'tp', swap)  9.21 us
  transfers between devices with their start and end apart: 37, of which 12 were waited for; matrix products, arithmetic and copies ran while one was open for 18% of the time, Pallas kernels for 10%

commit v1 on v0

--- a/solution.py
+++ b/solution.py
@@ -13,7 +13,8 @@
 LANES = 128
 CHUNK = 32
 HALO = 8
-GROUPS = ((6, "zx"), (5, "xz"))
+GROUPS = ((7, "zx"), (4, "xz"))
+GATHERS = ((6, "zx"), (5, "xz"))
 DIMS = {"y": 0, "z": 1, "x": 2}
 
 
@@ -52,9 +53,54 @@
     return (own + two) + (one + three)
 
 
-def two_parts(taps):
-    high = lax.reduce_precision(taps, 8, 7)
-    return high.astype(jnp.bfloat16), (taps - high).astype(jnp.bfloat16)
+def tap_kernel(columns, width, scale, *refs):
+    out_ref, values = refs[-1], []
+    for ref in refs[:-1]:
+        rows = ref[...].astype(jnp.float32)
+        if rows.shape[0] > 8:
+            cut = rows.shape[0] // 2
+            both = rows[:cut] + rows[cut:]
+            pieces = [both[k : k + 8] for k in range(0, cut, 8)]
+            values.append(jnp.concatenate(pieces, axis=1)[:, :columns])
+        elif rows.shape[1] == 2 * columns:
+            values.append(rows[:, :columns] + rows[:, columns:])
+        else:
+            values.append(rows)
+    total = four(*values) if len(values) == SIDE else jnp.concatenate(values, axis=1)
+    if scale is not None:
+        out_ref[...] = total * scale
+        return
+    high = total.astype(jnp.bfloat16).astype(jnp.float32)
+    parts = [high, total - high]
+    if width == 2 * columns:
+        out_ref[...] = jnp.concatenate(parts, axis=1).astype(jnp.bfloat16)
+        return
+    count = out_ref.shape[0] // 16
+    if count * width > columns:
+        blank = jnp.zeros((8, count * width - columns), jnp.float32)
+        parts = [jnp.concatenate([part, blank], axis=1) for part in parts]
+    cuts = [part[:, k * width : (k + 1) * width] for part in parts for k in range(count)]
+    out_ref[...] = jnp.concatenate(cuts, axis=0).astype(jnp.bfloat16)
+
+
+def tap_rows(tails, rows, columns, width, scale=None):
+    count = 8 if width == 2 * columns else 16 * (-(-columns // width))
+    out = (8, columns) if scale is not None else (count, width)
+    kind = jnp.float32 if scale is not None else jnp.bfloat16
+
+    def spec(tail):
+        last = tail.shape[0] // rows - 1
+        return pl.BlockSpec((rows, tail.shape[1]), lambda j: (last, 0))
+
+    return pl.pallas_call(
+        functools.partial(tap_kernel, columns, width, scale),
+        grid=(1,),
+        in_specs=[spec(tail) for tail in tails],
+        out_specs=pl.BlockSpec(out, lambda j: (0, 0)),
+        out_shape=jax.ShapeDtypeStruct(out, kind),
+        cost_estimate=pl.CostEstimate(flops=100000, bytes_accessed=500000, transcendentals=0),
+        name="tap_rows",
+    )(*tails)
 
 
 def add_up(kept, arrived):
@@ -64,8 +110,47 @@
     total = four(*[head.astype(jnp.float32) for head in heads])
     tails = None
     if extra is not None:
-        tails = [extra] + [part[count:] for part in arrived]
+        tails = [extra] + arrived
     return total.astype(jnp.bfloat16).reshape(own.shape), tails
+
+
+def relay_out(value, extra, axis):
+    me, dim, width = place(axis), DIMS[axis], value.shape[-1]
+    own, right, opposite, left = [
+        lax.dynamic_slice_in_dim(value, (me + hop) % SIDE, 1, dim).reshape(-1, width)
+        for hop in range(SIDE)
+    ]
+    cut = own.shape[0] // 2
+    tail = [] if extra is None else [extra]
+    upward = jnp.concatenate([opposite[:cut], right[cut:]] + tail, axis=0)
+    downward = jnp.concatenate([opposite[cut:], left[:cut]] + tail, axis=0)
+    return upward, downward, (own, right[:cut], left[cut:], extra)
+
+
+def relay_on(kept, arrived):
+    _, right, left, extra = kept
+    cut = right.shape[0]
+    below, above = arrived
+    upward = (right.astype(jnp.float32) + below[:cut].astype(jnp.float32)).astype(jnp.bfloat16)
+    downward = (left.astype(jnp.float32) + above[:cut].astype(jnp.float32)).astype(jnp.bfloat16)
+    if extra is not None:
+        upward = jnp.concatenate([upward, below[2 * cut :]], axis=0)
+    return upward, downward
+
+
+def relay_sum(kept, arrived, later):
+    own, right, _, extra = kept
+    cut = right.shape[0]
+    below, above = arrived
+    top = own[:cut].astype(jnp.float32) + above[cut : 2 * cut].astype(jnp.float32)
+    bottom = own[cut:].astype(jnp.float32) + below[cut : 2 * cut].astype(jnp.float32)
+    top = top + later[0][:cut].astype(jnp.float32)
+    bottom = bottom + later[1].astype(jnp.float32)
+    total = jnp.concatenate([top.astype(jnp.bfloat16), bottom.astype(jnp.bfloat16)], axis=0)
+    tails = None
+    if extra is not None:
+        tails = [extra, below, above, later[0]]
+    return total, tails
 
 
 def gather_over(value, axis):
@@ -311,38 +396,39 @@
     whole_rows = jnp.concatenate([first, second], axis=0)
 
     where = jnp.full((1,), tp, jnp.int32)
-    stacked, low, groups, tap_sums = None, 0, [], []
-    for blocks, _ in GROUPS:
+    stacked, low, tap_sums, begun, extra = None, 0, [], [], None
+    for number, (blocks, order) in enumerate(GROUPS):
         group, stacked, taps = backward(
             where, pre_gate[0], pre_up[0], cotangent[0], taps_gate, taps_up, low, blocks, stacked
         )
         low += blocks
-        groups.append(group)
         tap_sums.append(taps)
-    taps = jnp.concatenate(tap_sums, axis=1)
-    wide = groups[0].shape[1]
-    taps = jnp.pad(taps, ((0, 0), (0, wide - columns)))
-    extra = jnp.concatenate(two_parts(taps), axis=0)
-
-    begun = []
-    for group, (_, order) in zip(groups, GROUPS):
+        width = group.shape[1]
+        if number == len(GROUPS) - 1:
+            extra = tap_rows(tap_sums, 8, columns, width)
+            tap_count = extra.shape[0]
         value = jnp.einsum("nd,nk->dk", whole_rows, group, preferred_element_type=jnp.float32)
-        value = value.astype(jnp.bfloat16).reshape(SIDE, SIDE, SIDE, share, group.shape[1])
-        sent, kept = parts_for(value, extra, order[0])
+        value = value.astype(jnp.bfloat16).reshape(SIDE, SIDE, SIDE, share, width)
+        upward, downward, kept = relay_out(value, extra, order[0])
+        arrived = shift(upward, order[0], 1), shift(downward, order[0], SIDE - 1)
+        upward, downward = relay_on(kept, arrived)
+        later = shift(upward, order[0], 1), shift(downward, order[0], SIDE - 1)
+        arrived, _ = lax.optimization_barrier((arrived, (upward, downward)))
+        begun.append((kept, arrived, later))
+
+    lower = lax.optimization_barrier(lax.optimization_barrier(tp) == 0)
+    south = lax.optimization_barrier(lax.optimization_barrier(tp) < 1)
+    upper = lax.optimization_barrier(lax.optimization_barrier(tp) == 1)
+
+    middle = []
+    for (kept, arrived, later), (_, order) in zip(begun, GROUPS):
+        total, tails = relay_sum(kept, arrived, later)
+        lengths = [SIDE, SIDE, SIDE, share, total.shape[-1]]
+        lengths[DIMS[order[0]]] = 1
         extra = None
-        begun.append((kept, exchange(sent, order[0])))
-
-    lower = lax.optimization_barrier(lax.optimization_barrier(tp) == 0)
-    upper = lax.optimization_barrier(lax.optimization_barrier(tp) == 1)
-
-    def folded(tails):
-        return four(*[t[:8].astype(jnp.float32) + t[8:].astype(jnp.float32) for t in tails])
-
-    middle = []
-    for (kept, arrived), (_, order) in zip(begun, GROUPS):
-        value, tails = add_up(kept, arrived)
-        extra = None if tails is None else jnp.concatenate(two_parts(folded(tails)), axis=0)
-        sent, kept = parts_for(value, extra, order[1])
+        if tails is not None:
+            extra = tap_rows(tails, tap_count, columns, total.shape[-1])
+        sent, kept = parts_for(total.reshape(lengths), extra, order[1])
         middle.append((kept, exchange(sent, order[1])))
 
     values = []
@@ -350,35 +436,32 @@
         value, tails = add_up(kept, arrived)
         values.append(value.reshape(SIDE, 1, 1, share, value.shape[-1]))
         if tails is not None:
-            taps = folded(tails)[:, :columns]
+            extra = tap_rows(tails, tap_count, columns, 2 * columns)
     both = jnp.concatenate(values, axis=-1)
-    sent, kept = parts_for(both, jnp.concatenate(two_parts(taps), axis=1), "y")
+    sent, kept = parts_for(both, extra, "y")
     arrived = exchange(sent, "y")
     value, tails = add_up(kept, arrived)
     value = value.reshape(share, 2 * columns)
-    taps = four(
-        *[t[:, :columns].astype(jnp.float32) + t[:, columns:].astype(jnp.float32) for t in tails]
-    )
+    taps = tap_rows(tails, 8, columns, 2 * columns, factor)
 
     low, plan, pieces, parts = 0, [], [], []
-    for blocks, order in GROUPS:
+    for blocks, order in GATHERS:
         part = value[:, 2 * LANES * low : 2 * LANES * (low + blocks)]
         parts.append(gather_over(part, order[0]))
         plan.append((low, order[1], (0,) + HOPS))
         low += blocks
-    for part, (_, order) in zip(parts, GROUPS):
+    for part, (_, order) in zip(parts, GATHERS):
         pieces += [part] + exchange([part] * 3, order[1])
     places = jnp.stack([place("z"), place("x")]).astype(jnp.int32)
     grads = finish(places, tuple(plan), pieces, columns, factor)
     grads = [g.reshape(reps * share, columns) for g in grads]
 
-    taps = taps * factor
     other_taps = lax.ppermute(taps, "tp", swap)
     grad_taps = [
-        jnp.concatenate([jnp.where(ours, t, o), jnp.where(ours, o, t)], axis=1)
-        for ours, t, o in (
-            (lower, taps[:3], other_taps[:3]),
-            (jnp.logical_not(upper), taps[3:6], other_taps[3:6]),
+        jnp.concatenate([jnp.where(left, t, o), jnp.where(right, o, t)], axis=1)
+        for left, right, t, o in (
+            (lower, south, taps[:3], other_taps[:3]),
+            (jnp.logical_not(upper), jnp.logical_not(upper), taps[3:6], other_taps[3:6]),
         )
     ]
 

time: 231 us -> 250 us (1.082)
  the two profiles are of different devices: /device:TPU:1 before, /device:TPU:26 now
where the time goes in v1:
time: 250 us; the launch traced here: 249 us
  waiting for transfers between devices  103 us (41%)
  starting transfers between devices  45.4 us (18%)
  Pallas kernels  36.3 us (15%)
  matrix products  28.8 us (12%)
  other arithmetic  19.2 us (8%)
  local copies, waits for them, and re-layouts  15.4 us (6%)
    ppermute x26, waiting for transfers between devices, shift(): return lax.ppermute(value, 'rep', pairs)  73.9 us
    ppermute x26, starting transfers between devices, shift(): return lax.ppermute(value, 'rep', pairs)  36.9 us
    ppermute x7, waiting for transfers between devices, shift(): return lax.ppermute(value, 'fs', [(i, (i + hop) % SIDE) for i in ring])  28.9 us
    dot_general x5, matrix products, project(): jnp.einsum('nk,dk->nd', stacked, w, preferred_element_type=jnp.float32)  18.7 us
    pallas_call x2, Pallas kernels, backward(): pl.pallas_call(backward_kernel, grid_spec=pltpu.PrefetchScalarGridSpec(nu...  18.2 us
    dot_general x2, matrix products, layer(): jnp.einsum('nd,nk->dk', whole_rows, group, preferred_element_type=jnp.flo...  10 us
    ppermute x7, starting transfers between devices, shift(): return lax.ppermute(value, 'fs', [(i, (i + hop) % SIDE) for i in ring])  7.8 us
    pallas_call x4, Pallas kernels, tap_rows(): pl.pallas_call(functools.partial(tap_kernel, columns, width, scale), grid...  6.15 us
  transfers between devices with their start and end apart: 39, of which 16 were waited for; matrix products, arithmetic and copies ran while one was open for 24% of the time, Pallas kernels for 13%

profile of v1, /device:TPU:26, one launch (start us, length us, event | category | flops | bytes accessed | tf_op | source)
XLA Modules:
  0.0 249.2 jit_solution(8747830200723103788)
XLA Ops:
  0.7 4.2 %weave.1 = bf16[512,2816]{1,0:T(8,128)(2,1)} custom-call(bf16[512,1408]{1,0:T(8,128)(2,1)} %gate_ref.1, bf16[512,1408]{1,0:T(8,128)(2,1)} %up_ref.1), custom_call_target="tpu_custom_call" | custom-call | flops 72089600 | bytes 5767168 | tf_op jit(solution)/shard_map/weave/pallas_call | solution.py:272
  7.0 11.0 %backward.2 = (bf16[768,1792]{1,0:T(8,128)(2,1)}, bf16[768,2816]{1,0:T(8,128)(2,1)}, f32[8,896]{1,0:T(8,128)}) custom-call(s32[1]{0:T(128)} %bitcast.1.tp_ref, bf16[768,1408]{1,0:T(8,128)(2,1)} %bitcast.114, bf16[768,1408]{1,0:T(8,128)(2,1)} %bitcast.116, bf16[768,1408]{1,0:T(8,128)(2,1)} %bitcast.118, bf16[3,2816]{1,0:T(4,128)(2,1)} %tap_gate_ref.3, ...), custom_call_target="tpu_custom_call" | custom-call | flops 1376256000 | bytes 9633792 | tf_op jit(solution)/shard_map/backward/pallas_call | solution.py:234
  18.0 7.2 %backward.3 = (bf16[768,1024]{1,0:T(8,128)(2,1)}, bf16[768,2816]{1,0:T(8,128)(2,1)}, f32[8,512]{1,0:T(8,128)}) custom-call(s32[1]{0:T(128)} %bitcast.1.tp_ref, bf16[768,1408]{1,0:T(8,128)(2,1)} %bitcast.115, bf16[768,1408]{1,0:T(8,128)(2,1)} %bitcast.117, bf16[768,1408]{1,0:T(8,128)(2,1)} %bitcast.119, ...), custom_call_target="tpu_custom_call", output_to_operand_aliasing={{1}: (6, {})} | custom-call | flops 786432000 | bytes 5505024 | tf_op jit(solution)/shard_map/backward/pallas_call | solution.py:234
  25.2 4.6 %convolution_convert_fusion.4 = bf16[768,512]{1,0:T(8,128)(2,1)S(1)} fusion(bf16[768,2816]{1,0:T(8,128)(2,1)} %get-tuple-element.18, bf16[512,2816]{1,0:T(8,128)(2,1)S(1)} %copy-done.4), kind=kOutput, calls=%fused_computation.22 | convolution fusion | flops 2214985728 | bytes 7995392 | tf_op jit(solution)/shard_map/nk,dk->nd/dot_general | solution.py:469
  34.2 3.7 %convolution_convert_fusion.1 = bf16[2048,1024]{1,0:T(8,128)(2,1)S(1)} fusion(bf16[768,1024]{1,0:T(8,128)(2,1)S(1)} %copy-done.31, bf16[384,2048]{1,0:T(8,128)(2,1)S(1)} %get-tuple-element.46, bf16[384,2048]{1,0:T(8,128)(2,1)S(1)} %get-tuple-element.45), kind=kOutput, calls=%fused_computation.1 | convolution fusion | flops 3229614080 | bytes 8912896 | tf_op jit(solution)/shard_map/nd,nk->dk/dot_general | solution.py:410
  40.6 6.3 %convolution_convert_fusion = bf16[2048,1792]{1,0:T(8,128)(2,1)S(1)} fusion(bf16[768,1792]{1,0:T(8,128)(2,1)S(1)} %copy-done.30, bf16[384,2048]{1,0:T(8,128)(2,1)S(1)} %get-tuple-element.46, bf16[384,2048]{1,0:T(8,128)(2,1)S(1)} %get-tuple-element.45), kind=kOutput, calls=%fused_computation | convolution fusion | flops 5647106048 | bytes 13238272 | tf_op jit(solution)/shard_map/nd,nk->dk/dot_general | solution.py:410
  52.1 13.9 %collective-permute-done.16.refs_1_ = bf16[544,1024]{1,0:T(8,128)(2,1)S(1)} collective-permute-done((bf16[544,1024]{1,0:T(8,128)(2,1)S(1)}, bf16[544,1024]{1,0:T(8,128)(2,1)S(1)}, u32[]{:S(2)}, u32[]{:S(2)}) %collective-permute-start.16) | collective-permute-done | bytes 1114144 | tf_op jit(solution)/shard_map/ppermute | solution.py:29
  66.0 4.0 %collective-permute-start.10 = (bf16[512,1792]{1,0:T(8,128)(2,1)}, bf16[512,1792]{1,0:T(8,128)(2,1)}, u32[]{:S(2)}, u32[]{:S(2)}) collective-permute-start(bf16[512,1792]{1,0:T(8,128)(2,1)} %pad_maximum_fusion.4), channel_id=1, source_target_pairs={{0,96},{8,104},{16,112},{24,120},{32,0},{40,8},{48,16},{56,24},{64... | collective-permute-start | bytes 5505032 | tf_op jit(solution)/shard_map/ppermute | solution.py:29
  70.4 3.6 %collective-permute-done.17.refs_2_ = bf16[544,1024]{1,0:T(8,128)(2,1)S(1)} collective-permute-done((bf16[544,1024]{1,0:T(8,128)(2,1)S(1)}, bf16[544,1024]{1,0:T(8,128)(2,1)S(1)}, u32[]{:S(2)}, u32[]{:S(2)}) %collective-permute-start.17) | collective-permute-done | bytes 1114144 | tf_op jit(solution)/shard_map/ppermute | solution.py:29
  77.7 4.2 %convolution_convert_fusion.3 = bf16[768,512]{1,0:T(8,128)(2,1)S(1)} fusion(bf16[768,2816]{1,0:T(8,128)(2,1)S(1)} %bitcast.123, bf16[512,2816]{1,0:T(8,128)(2,1)} %collective-permute-done), kind=kOutput, calls=%fused_computation.21 | convolution fusion | flops 2214985728 | bytes 7995392 | tf_op jit(solution)/shard_map/nk,dk->nd/dot_general | solution.py:469
  82.5 4.2 %convolution_convert_fusion.2 = bf16[768,512]{1,0:T(8,128)(2,1)S(1)} fusion(bf16[768,2816]{1,0:T(8,128)(2,1)S(1)} %bitcast.123, bf16[512,2816]{1,0:T(8,128)(2,1)} %collective-permute-done.1), kind=kOutput, calls=%fused_computation.20 | convolution fusion | flops 2214985728 | bytes 7995392 | tf_op jit(solution)/shard_map/nk,dk->nd/dot_general | solution.py:469
  101.3 8.3 %collective-permute-done.10 = bf16[512,1792]{1,0:T(8,128)(2,1)} collective-permute-done((bf16[512,1792]{1,0:T(8,128)(2,1)}, bf16[512,1792]{1,0:T(8,128)(2,1)}, u32[]{:S(2)}, u32[]{:S(2)}) %collective-permute-start.10) | collective-permute-done | bytes 1835040 | tf_op jit(solution)/shard_map/ppermute | solution.py:29
  111.0 3.8 %collective-permute-start.12 = (bf16[256,1792]{1,0:T(8,128)(2,1)S(1)}, bf16[256,1792]{1,0:T(8,128)(2,1)S(1)}, u32[]{:S(2)}, u32[]{:S(2)}) collective-permute-start(bf16[256,1792]{1,0:T(8,128)(2,1)S(1)} %fusion.2), channel_id=1, source_target_pairs={{0,96},{8,104},{16,112},{24,120},{32,0},{40,8},{48,16},{56,24},{64... | collective-permute-start | bytes 2752520 | tf_op jit(solution)/shard_map/ppermute | solution.py:29
  114.8 3.5 %collective-permute-done.9 = bf16[512,1792]{1,0:T(8,128)(2,1)} collective-permute-done((bf16[512,1792]{1,0:T(8,128)(2,1)}, bf16[512,1792]{1,0:T(8,128)(2,1)}, u32[]{:S(2)}, u32[]{:S(2)}) %collective-permute-start.9) | collective-permute-done | bytes 1835040 | tf_op jit(solution)/shard_map/ppermute | solution.py:29
  123.3 12.2 %collective-permute-done.12 = bf16[256,1792]{1,0:T(8,128)(2,1)S(1)} collective-permute-done((bf16[256,1792]{1,0:T(8,128)(2,1)S(1)}, bf16[256,1792]{1,0:T(8,128)(2,1)S(1)}, u32[]{:S(2)}, u32[]{:S(2)}) %collective-permute-start.12) | collective-permute-done | bytes 917536 | tf_op jit(solution)/shard_map/ppermute | solution.py:29
  137.1 7.0 %collective-permute-done.11 = bf16[256,1792]{1,0:T(8,128)(2,1)S(1)} collective-permute-done((bf16[256,1792]{1,0:T(8,128)(2,1)S(1)}, bf16[256,1792]{1,0:T(8,128)(2,1)S(1)}, u32[]{:S(2)}, u32[]{:S(2)}) %collective-permute-start.11) | collective-permute-done | bytes 917536 | tf_op jit(solution)/shard_map/ppermute | solution.py:29
  148.2 8.2 %collective-permute-done.21.refs_1_ = bf16[160,1024]{1,0:T(8,128)(2,1)S(1)} collective-permute-done((bf16[160,1024]{1,0:T(8,128)(2,1)S(1)}, bf16[160,1024]{1,0:T(8,128)(2,1)S(1)}, u32[]{:S(2)}, u32[]{:S(2)}) %collective-permute-start.21) | collective-permute-done | bytes 327712 | tf_op jit(solution)/shard_map/ppermute | solution.py:29
  162.5 4.3 %convolution_convert_fusion.6 = bf16[768,256]{1,0:T(8,128)(2,1)S(1)} fusion(bf16[768,2816]{1,0:T(8,128)(2,1)} %get-tuple-element.18, bf16[256,2816]{1,0:T(8,128)(2,1)} %collective-permute-done.2), kind=kOutput, calls=%fused_computation.24 | convolution fusion | flops 1107492864 | bytes 6160384 | tf_op jit(solution)/shard_map/nk,dk->nd/dot_general | solution.py:469
  173.7 24.1 %collective-permute-done.3 = bf16[256,2816]{1,0:T(8,128)(2,1)S(1)} collective-permute-done((bf16[256,2816]{1,0:T(8,128)(2,1)S(1)}, bf16[256,2816]{1,0:T(8,128)(2,1)S(1)}, u32[]{:S(2)}, u32[]{:S(2)}) %collective-permute-start.3) | collective-permute-done | bytes 1441824 | tf_op jit(solution)/shard_map/ppermute | solution.py:24
  201.6 3.6 %collective-permute-done.23.refs_3_ = bf16[40,2816]{1,0:T(8,128)(2,1)S(1)} collective-permute-done((bf16[40,2816]{1,0:T(8,128)(2,1)S(1)}, bf16[40,2816]{1,0:T(8,128)(2,1)S(1)}, u32[]{:S(2)}, u32[]{:S(2)}) %collective-permute-start.23) | collective-permute-done | bytes 225312 | tf_op jit(solution)/shard_map/ppermute | solution.py:24
  211.1 3.2 %join.1 = bf16[384,2048]{1,0:T(8,128)(2,1)} custom-call(s32[1]{0:T(128)} %bitcast.place_ref, bf16[384,512]{1,0:T(8,128)(2,1)} %get-tuple-element.62.refs_0_, bf16[384,512]{1,0:T(8,128)(2,1)} %get-tuple-element.60.refs_1_, bf16[384,512]{1,0:T(8,128)(2,1)} %get-tuple-element.58.refs_2_, bf16[384,512]{1,0:T(8,128)(2,1)} %get-tuple-element.56.refs_3_, ...), custom_call_target="tpu_custom_call" | custom-call | flops 78643200 | bytes 4718592 | tf_op jit(solution)/shard_map/join/pallas_call | solution.py:304
  220.6 3.3 %collective-permute-done.26 = bf16[32,1536]{1,0:T(8,128)(2,1)S(1)} collective-permute-done((bf16[32,1536]{1,0:T(8,128)(2,1)S(1)}, bf16[32,1536]{1,0:T(8,128)(2,1)S(1)}, u32[]{:S(2)}, u32[]{:S(2)}) %collective-permute-start.26) | collective-permute-done | bytes 98336 | tf_op jit(solution)/shard_map/ppermute | solution.py:29
  233.1 9.6 %collective-permute-done.36.refs_6_ = bf16[4,32,1280]{2,1,0:T(8,128)(2,1)S(1)} collective-permute-done((bf16[4,32,1280]{2,1,0:T(8,128)(2,1)S(1)}, bf16[4,32,1280]{2,1,0:T(8,128)(2,1)S(1)}, u32[]{:S(2)}, u32[]{:S(2)}) %collective-permute-start.36) | collective-permute-done | bytes 327712 | tf_op jit(solution)/shard_map/ppermute | solution.py:29
  244.5 4.5 %finish.1 = (f32[4,4,32,1408]{3,2,1,0:T(8,128)}, f32[4,4,32,1408]{3,2,1,0:T(8,128)}) custom-call(s32[2]{0:T(128)} %pad_add_fusion.places, bf16[4,32,1536]{2,1,0:T(8,128)(2,1)} %copy-done.6, bf16[4,32,1536]{2,1,0:T(8,128)(2,1)} %copy-done.20, bf16[4,32,1536]{2,1,0:T(8,128)(2,1)} %copy-done.22, bf16[4,32,1536]{2,1,0:T(8,128)(2,1)} %copy-done.23, ...), custom_call_target="tpu_custom_call" | custom-call | flops 144179200 | bytes 8650752 | tf_op jit(solution)/shard_map/finish/pallas_call | solution.py:361
  (187 shorter events, 85.1 us)
Async XLA Ops:
  0.6 31.7 %collective-permute-start.8 = (bf16[384,2048]{1,0:T(8,128)(2,1)}, bf16[384,2048]{1,0:T(8,128)(2,1)}, u32[]{:S(2)}, u32[]{:S(2)}) collective-permute-start(bf16[384,2048]{1,0:T(8,128)(2,1)} %bitcast.141), channel_id=1, source_target_pairs={{0,1},{1,0},{2,3},{3,2},{4,5},{5,4},{6,7},{7,6},{8,9},{9,8},{10,11... | collective-permute-start | bytes 4718600 | tf_op jit(solution)/shard_map/ppermute | solution.py:393
  4.9 71.1 %collective-permute-start = (bf16[512,2816]{1,0:T(8,128)(2,1)}, bf16[512,2816]{1,0:T(8,128)(2,1)}, u32[]{:S(2)}, u32[]{:S(2)}) collective-permute-start(bf16[512,2816]{1,0:T(8,128)(2,1)} %weave.1), channel_id=1, source_target_pairs={{0,2},{2,4},{4,6},{6,0},{1,3},{3,5},{5,7},{7,1},{8,10},{10,12},{12... | collective-permute-start | bytes 8650760 | tf_op jit(solution)/shard_map/ppermute | solution.py:24
  5.2 76.7 %collective-permute-start.1 = (bf16[512,2816]{1,0:T(8,128)(2,1)}, bf16[512,2816]{1,0:T(8,128)(2,1)}, u32[]{:S(2)}, u32[]{:S(2)}) collective-permute-start(bf16[512,2816]{1,0:T(8,128)(2,1)} %weave.1), channel_id=1, source_target_pairs={{0,6},{2,0},{4,2},{6,4},{1,7},{3,1},{5,3},{7,5},{8,14},{10,8},{12,... | collective-permute-start | bytes 8650760 | tf_op jit(solution)/shard_map/ppermute | solution.py:24
  30.9 175.7 %collective-permute-start.4 = (bf16[384,512]{1,0:T(8,128)(2,1)}, bf16[384,512]{1,0:T(8,128)(2,1)}, u32[]{:S(2)}, u32[]{:S(2)}) collective-permute-start(bf16[384,512]{1,0:T(8,128)(2,1)} %get-tuple-element.61), channel_id=1, source_target_pairs={{0,1},{1,0},{2,3},{3,2},{4,5},{5,4},{6,7},{7,6},{8,9},{9,8},{10,11... | collective-permute-start | bytes 1179656 | tf_op jit(solution)/shard_map/ppermute | solution.py:476
  39.0 27.0 %collective-permute-start.16 = (bf16[544,1024]{1,0:T(8,128)(2,1)S(1)}, bf16[544,1024]{1,0:T(8,128)(2,1)S(1)}, u32[]{:S(2)}, u32[]{:S(2)}) collective-permute-start(bf16[544,1024]{1,0:T(8,128)(2,1)S(1)} %get-tuple-element.74), channel_id=1, source_target_pairs={{0,8},{8,16},{16,24},{24,0},{32,40},{40,48},{48,56},{56,32},{64,72... | collective-permute-start | bytes 3342344 | tf_op jit(solution)/shard_map/ppermute | solution.py:29
  46.9 27.0 %collective-permute-start.17 = (bf16[544,1024]{1,0:T(8,128)(2,1)S(1)}, bf16[544,1024]{1,0:T(8,128)(2,1)S(1)}, u32[]{:S(2)}, u32[]{:S(2)}) collective-permute-start(bf16[544,1024]{1,0:T(8,128)(2,1)S(1)} %get-tuple-element.73), channel_id=1, source_target_pairs={{0,24},{8,0},{16,8},{24,16},{32,56},{40,32},{48,40},{56,48},{64,88... | collective-permute-start | bytes 3342344 | tf_op jit(solution)/shard_map/ppermute | solution.py:29
  66.0 43.5 %collective-permute-start.10 = (bf16[512,1792]{1,0:T(8,128)(2,1)}, bf16[512,1792]{1,0:T(8,128)(2,1)}, u32[]{:S(2)}, u32[]{:S(2)}) collective-permute-start(bf16[512,1792]{1,0:T(8,128)(2,1)} %pad_maximum_fusion.4), channel_id=1, source_target_pairs={{0,96},{8,104},{16,112},{24,120},{32,0},{40,8},{48,16},{56,24},{64... | collective-permute-start | bytes 5505032 | tf_op jit(solution)/shard_map/ppermute | solution.py:29
  73.9 44.3 %collective-permute-start.9 = (bf16[512,1792]{1,0:T(8,128)(2,1)}, bf16[512,1792]{1,0:T(8,128)(2,1)}, u32[]{:S(2)}, u32[]{:S(2)}) collective-permute-start(bf16[512,1792]{1,0:T(8,128)(2,1)} %pad_maximum_fusion.3), channel_id=1, source_target_pairs={{0,32},{8,40},{16,48},{24,56},{32,64},{40,72},{48,80},{56,88},{64,... | collective-permute-start | bytes 5505032 | tf_op jit(solution)/shard_map/ppermute | solution.py:29
  76.1 22.0 %collective-permute-start.18 = (bf16[288,1024]{1,0:T(8,128)(2,1)S(1)}, bf16[288,1024]{1,0:T(8,128)(2,1)}, u32[]{:S(2)}, u32[]{:S(2)}) collective-permute-start(bf16[288,1024]{1,0:T(8,128)(2,1)S(1)} %pad_maximum_fusion.9), channel_id=1, source_target_pairs={{0,8},{8,16},{16,24},{24,0},{32,40},{40,48},{48,56},{56,32},{64,72... | collective-permute-start | bytes 1769480 | tf_op jit(solution)/shard_map/ppermute | solution.py:29
  95.6 66.1 %collective-permute-start.2 = (bf16[256,2816]{1,0:T(8,128)(2,1)}, bf16[256,2816]{1,0:T(8,128)(2,1)}, u32[]{:S(2)}, u32[]{:S(2)}) collective-permute-start(bf16[256,2816]{1,0:T(8,128)(2,1)} %slice.200), channel_id=1, source_target_pairs={{0,2},{2,4},{4,6},{6,0},{1,3},{3,5},{5,7},{7,1},{8,10},{10,12},{12... | collective-permute-start | bytes 4325384 | tf_op jit(solution)/shard_map/ppermute | solution.py:24
  111.0 24.5 %collective-permute-start.12 = (bf16[256,1792]{1,0:T(8,128)(2,1)S(1)}, bf16[256,1792]{1,0:T(8,128)(2,1)S(1)}, u32[]{:S(2)}, u32[]{:S(2)}) collective-permute-start(bf16[256,1792]{1,0:T(8,128)(2,1)S(1)} %fusion.2), channel_id=1, source_target_pairs={{0,96},{8,104},{16,112},{24,120},{32,0},{40,8},{48,16},{56,24},{64... | collective-permute-start | bytes 2752520 | tf_op jit(solution)/shard_map/ppermute | solution.py:29
  119.6 24.5 %collective-permute-start.11 = (bf16[256,1792]{1,0:T(8,128)(2,1)S(1)}, bf16[256,1792]{1,0:T(8,128)(2,1)S(1)}, u32[]{:S(2)}, u32[]{:S(2)}) collective-permute-start(bf16[256,1792]{1,0:T(8,128)(2,1)S(1)} %fusion.3), channel_id=1, source_target_pairs={{0,32},{8,40},{16,48},{24,56},{32,64},{40,72},{48,80},{56,88},{64,... | collective-permute-start | bytes 2752520 | tf_op jit(solution)/shard_map/ppermute | solution.py:29
  120.5 26.9 %collective-permute-start.22 = (bf16[160,1024]{1,0:T(8,128)(2,1)S(1)}, bf16[160,1024]{1,0:T(8,128)(2,1)S(1)}, u32[]{:S(2)}, u32[]{:S(2)}) collective-permute-start(bf16[160,1024]{1,0:T(8,128)(2,1)S(1)} %get-tuple-element.72), channel_id=1, source_target_pairs={{0,96},{8,104},{16,112},{24,120},{32,0},{40,8},{48,16},{56,24},{64... | collective-permute-start | bytes 983048 | tf_op jit(solution)/shard_map/ppermute | solution.py:29
  135.5 20.9 %collective-permute-start.21 = (bf16[160,1024]{1,0:T(8,128)(2,1)S(1)}, bf16[160,1024]{1,0:T(8,128)(2,1)S(1)}, u32[]{:S(2)}, u32[]{:S(2)}) collective-permute-start(bf16[160,1024]{1,0:T(8,128)(2,1)S(1)} %get-tuple-element.71), channel_id=1, source_target_pairs={{0,32},{8,40},{16,48},{24,56},{32,64},{40,72},{48,80},{56,88},{64,... | collective-permute-start | bytes 983048 | tf_op jit(solution)/shard_map/ppermute | solution.py:29
  144.1 13.8 %collective-permute-start.20 = (bf16[160,1024]{1,0:T(8,128)(2,1)S(1)}, bf16[160,1024]{1,0:T(8,128)(2,1)S(1)}, u32[]{:S(2)}, u32[]{:S(2)}) collective-permute-start(bf16[160,1024]{1,0:T(8,128)(2,1)S(1)} %get-tuple-element.70), channel_id=1, source_target_pairs={{0,64},{8,72},{16,80},{24,88},{32,96},{40,104},{48,112},{56,120},{... | collective-permute-start | bytes 983048 | tf_op jit(solution)/shard_map/ppermute | solution.py:29
  147.4 19.4 %collective-permute-start.15 = (bf16[128,1792]{1,0:T(8,128)(2,1)}, bf16[128,1792]{1,0:T(8,128)(2,1)}, u32[]{:S(2)}, u32[]{:S(2)}) collective-permute-start(bf16[128,1792]{1,0:T(8,128)(2,1)} %bitcast.22), channel_id=1, source_target_pairs={{0,24},{8,0},{16,8},{24,16},{32,56},{40,32},{48,40},{56,48},{64,88... | collective-permute-start | bytes 1376264 | tf_op jit(solution)/shard_map/ppermute | solution.py:29
  161.6 36.1 %collective-permute-start.3 = (bf16[256,2816]{1,0:T(8,128)(2,1)S(1)}, bf16[256,2816]{1,0:T(8,128)(2,1)S(1)}, u32[]{:S(2)}, u32[]{:S(2)}) collective-permute-start(bf16[256,2816]{1,0:T(8,128)(2,1)S(1)} %copy-done.8), channel_id=1, source_target_pairs={{0,6},{2,0},{4,2},{6,4},{1,7},{3,1},{5,3},{7,5},{8,14},{10,8},{12,... | collective-permute-start | bytes 4325384 | tf_op jit(solution)/shard_map/ppermute | solution.py:24
  166.8 40.3 %collective-permute-start.5 = (bf16[384,512]{1,0:T(8,128)(2,1)S(1)}, bf16[384,512]{1,0:T(8,128)(2,1)S(1)}, u32[]{:S(2)}, u32[]{:S(2)}) collective-permute-start(bf16[384,512]{1,0:T(8,128)(2,1)S(1)} %copy-done.26), channel_id=1, source_target_pairs={{0,1},{1,0},{2,3},{3,2},{4,5},{5,4},{6,7},{7,6},{8,9},{9,8},{10,11... | collective-permute-start | bytes 1179656 | tf_op jit(solution)/shard_map/ppermute | solution.py:476
  170.1 30.9 %collective-permute-start.25 = (bf16[40,2816]{1,0:T(8,128)(2,1)S(1)}, bf16[40,2816]{1,0:T(8,128)(2,1)S(1)}, u32[]{:S(2)}, u32[]{:S(2)}) collective-permute-start(bf16[40,2816]{1,0:T(8,128)(2,1)S(1)} %get-tuple-element.77), channel_id=1, source_target_pairs={{0,6},{2,0},{4,2},{6,4},{1,7},{3,1},{5,3},{7,5},{8,14},{10,8},{12,... | collective-permute-start | bytes 675848 | tf_op jit(solution)/shard_map/ppermute | solution.py:24
  171.2 29.9 %collective-permute-start.24 = (bf16[40,2816]{1,0:T(8,128)(2,1)S(1)}, bf16[40,2816]{1,0:T(8,128)(2,1)S(1)}, u32[]{:S(2)}, u32[]{:S(2)}) collective-permute-start(bf16[40,2816]{1,0:T(8,128)(2,1)S(1)} %get-tuple-element.76), channel_id=1, source_target_pairs={{0,2},{2,4},{4,6},{6,0},{1,3},{3,5},{5,7},{7,1},{8,10},{10,12},{12... | collective-permute-start | bytes 675848 | tf_op jit(solution)/shard_map/ppermute | solution.py:24
  224.1 18.6 %collective-permute-start.29 = (bf16[4,32,1536]{2,1,0:T(8,128)(2,1)S(1)}, bf16[4,32,1536]{2,1,0:T(8,128)(2,1)S(1)}, u32[]{:S(2)}, u32[]{:S(2)}) collective-permute-start(bf16[4,32,1536]{2,1,0:T(8,128)(2,1)S(1)} %select_select_fusion.refs_0_), channel_id=1, source_target_pairs={{0,8},{8,16},{16,24},{24,0},{32,40},{40,48},{48,56},{56,32},{64,72... | collective-permute-start | bytes 1179656 | tf_op jit(solution)/shard_map/ppermute | solution.py:29
  225.2 17.5 %collective-permute-start.30 = (bf16[4,32,1536]{2,1,0:T(8,128)(2,1)S(1)}, bf16[4,32,1536]{2,1,0:T(8,128)(2,1)S(1)}, u32[]{:S(2)}, u32[]{:S(2)}) collective-permute-start(bf16[4,32,1536]{2,1,0:T(8,128)(2,1)S(1)} %select_select_fusion.refs_0_), channel_id=1, source_target_pairs={{0,24},{8,0},{16,8},{24,16},{32,56},{40,32},{48,40},{56,48},{64,88... | collective-permute-start | bytes 1179656 | tf_op jit(solution)/shard_map/ppermute | solution.py:29
  226.2 16.6 %collective-permute-start.31 = (bf16[4,32,1536]{2,1,0:T(8,128)(2,1)S(1)}, bf16[4,32,1536]{2,1,0:T(8,128)(2,1)S(1)}, u32[]{:S(2)}, u32[]{:S(2)}) collective-permute-start(bf16[4,32,1536]{2,1,0:T(8,128)(2,1)S(1)} %select_select_fusion.refs_0_), channel_id=1, source_target_pairs={{0,16},{8,24},{16,0},{24,8},{32,48},{40,56},{48,32},{56,40},{64,80... | collective-permute-start | bytes 1179656 | tf_op jit(solution)/shard_map/ppermute | solution.py:29
  229.0 13.7 %collective-permute-start.36 = (bf16[4,32,1280]{2,1,0:T(8,128)(2,1)S(1)}, bf16[4,32,1280]{2,1,0:T(8,128)(2,1)S(1)}, u32[]{:S(2)}, u32[]{:S(2)}) collective-permute-start(bf16[4,32,1280]{2,1,0:T(8,128)(2,1)S(1)} %select_select_fusion.1.refs_4_), channel_id=1, source_target_pairs={{0,96},{8,104},{16,112},{24,120},{32,0},{40,8},{48,16},{56,24},{64... | collective-permute-start | bytes 983048 | tf_op jit(solution)/shard_map/ppermute | solution.py:29
  (51 other events, 513.5 us)

commit v2 on v1

--- a/solution.py
+++ b/solution.py
@@ -13,7 +13,7 @@
 LANES = 128
 CHUNK = 32
 HALO = 8
-GROUPS = ((7, "zx"), (4, "xz"))
+GROUPS = ((6, "zx"), (5, "xz"))
 GATHERS = ((6, "zx"), (5, "xz"))
 DIMS = {"y": 0, "z": 1, "x": 2}
 
@@ -99,6 +99,7 @@
         out_specs=pl.BlockSpec(out, lambda j: (0, 0)),
         out_shape=jax.ShapeDtypeStruct(out, kind),
         cost_estimate=pl.CostEstimate(flops=100000, bytes_accessed=500000, transcendentals=0),
+        compiler_params=pltpu.CompilerParams(vmem_limit_bytes=4 * 1024 * 1024),
         name="tap_rows",
     )(*tails)
 
@@ -255,6 +256,7 @@
             bytes_accessed=length * LANES * blocks * 14,
             transcendentals=length * LANES * blocks,
         ),
+        compiler_params=pltpu.CompilerParams(vmem_limit_bytes=16 * 1024 * 1024),
         name="backward",
     )(*operands)
 
@@ -278,6 +280,7 @@
         cost_estimate=pl.CostEstimate(
             flops=100 * rows * columns, bytes_accessed=8 * rows * columns, transcendentals=0
         ),
+        compiler_params=pltpu.CompilerParams(vmem_limit_bytes=8 * 1024 * 1024),
         name="weave",
     )(gate, up)
 
@@ -314,6 +317,7 @@
         cost_estimate=pl.CostEstimate(
             flops=400 * rows * width, bytes_accessed=24 * rows * width, transcendentals=0
         ),
+        compiler_params=pltpu.CompilerParams(vmem_limit_bytes=10 * 1024 * 1024),
         name="join",
     )(place_y, *kept, *got)
 
@@ -371,6 +375,7 @@
         cost_estimate=pl.CostEstimate(
             flops=200 * size, bytes_accessed=12 * size, transcendentals=0
         ),
+        compiler_params=pltpu.CompilerParams(vmem_limit_bytes=16 * 1024 * 1024),
         name="finish",
     )(places, *pieces)
 
@@ -418,6 +423,7 @@
 
     lower = lax.optimization_barrier(lax.optimization_barrier(tp) == 0)
     south = lax.optimization_barrier(lax.optimization_barrier(tp) < 1)
+    north = lax.optimization_barrier(lax.optimization_barrier(tp) > 0)
     upper = lax.optimization_barrier(lax.optimization_barrier(tp) == 1)
 
     middle = []
@@ -461,7 +467,7 @@
         jnp.concatenate([jnp.where(left, t, o), jnp.where(right, o, t)], axis=1)
         for left, right, t, o in (
             (lower, south, taps[:3], other_taps[:3]),
-            (jnp.logical_not(upper), jnp.logical_not(upper), taps[3:6], other_taps[3:6]),
+            (jnp.logical_not(upper), jnp.logical_not(north), taps[3:6], other_taps[3:6]),
         )
     ]
 

time: 250 us -> 231 us (0.924)
  the two profiles are of different devices: /device:TPU:26 before, /device:TPU:1 now
where the time goes in v2:
time: 231 us; the launch traced here: 230 us
  waiting for transfers between devices  91.1 us (39%)
  starting transfers between devices  67.8 us (29%)
  matrix products  27 us (12%)
  Pallas kernels  21.7 us (9%)
  local copies, waits for them, and re-layouts  13.6 us (6%)
  other arithmetic  6.95 us (3%)
    ppermute x26, waiting for transfers between devices, shift(): return lax.ppermute(value, 'rep', pairs)  69.4 us
    ppermute x26, starting transfers between devices, shift(): return lax.ppermute(value, 'rep', pairs)  39.1 us
    ppermute x7, waiting for transfers between devices, shift(): return lax.ppermute(value, 'fs', [(i, (i + hop) % SIDE) for i in ring])  21.7 us
    dot_general x5, matrix products, project(): jnp.einsum('nk,dk->nd', stacked, w, preferred_element_type=jnp.float32)  16.9 us
    ppermute x4, starting transfers between devices, layer(): got = [lax.ppermute(p, 'tp', swap) for p in away]  16.9 us
    pallas_call x2, Pallas kernels, backward(): pl.pallas_call(backward_kernel, grid_spec=pltpu.PrefetchScalarGridSpec(nu...  14.8 us
    dot_general x2, matrix products, layer(): jnp.einsum('nd,nk->dk', whole_rows, group, preferred_element_type=jnp.flo...  10.2 us
    unnamed x28, local copies, waits for them, and re-layouts  9.15 us
  transfers between devices with their start and end apart: 39, of which 15 were waited for; matrix products, arithmetic and copies ran while one was open for 17% of the time, Pallas kernels for 7%

profile of v2, /device:TPU:1, one launch (start us, length us, event | category | flops | bytes accessed | tf_op | source)
XLA Modules:
  0.0 229.9 jit_solution(4326159109742265551)
XLA Ops:
  13.6 8.0 %backward.2 = (bf16[768,1536]{1,0:T(8,128)(2,1)S(1)}, bf16[768,2816]{1,0:T(8,128)(2,1)S(1)}, f32[8,768]{1,0:T(8,128)S(1)}) custom-call(s32[1]{0:T(128)} %bitcast.1.tp_ref, bf16[768,1408]{1,0:T(8,128)(2,1)S(1)} %bitcast.114, bf16[768,1408]{1,0:T(8,128)(2,1)S(1)} %bitcast.116, bf16[768,1408]{1,0:T(8,128)(2,1)S(1)} %bitcast.118, bf16[3,2816]{1,0:T(4,128)(2,1)S(1)} %copy-done.6, ...), custom_call_target="tpu_custom_call" | custom-call | flops 1179648000 | bytes 8257536 | tf_op jit(solution)/shard_map/backward/pallas_call | solution.py:235
  21.6 6.7 %backward.3 = (bf16[768,1280]{1,0:T(8,128)(2,1)S(1)}, bf16[768,2816]{1,0:T(8,128)(2,1)S(1)}, f32[8,640]{1,0:T(8,128)S(1)}) custom-call(s32[1]{0:T(128)} %bitcast.1.tp_ref, bf16[768,1408]{1,0:T(8,128)(2,1)S(1)} %bitcast.115, bf16[768,1408]{1,0:T(8,128)(2,1)S(1)} %bitcast.117, bf16[768,1408]{1,0:T(8,128)(2,1)S(1)} %bitcast.119, ...), custom_call_target="tpu_custom_call", output_to_operand_aliasing={{1}: (6, {})} | custom-call | flops 983040000 | bytes 6881280 | tf_op jit(solution)/shard_map/backward/pallas_call | solution.py:235
  29.7 5.8 %convolution_convert_fusion.4 = bf16[768,512]{1,0:T(8,128)(2,1)S(1)} fusion(bf16[768,2816]{1,0:T(8,128)(2,1)S(1)} %get-tuple-element.18, bf16[512,2816]{1,0:T(8,128)(2,1)} %weave.1), kind=kOutput, calls=%fused_computation.22 | convolution fusion | flops 2214985728 | bytes 7995392 | tf_op jit(solution)/shard_map/nk,dk->nd/dot_general | solution.py:475
  38.7 5.5 %convolution_convert_fusion = bf16[2048,1536]{1,0:T(8,128)(2,1)S(1)} fusion(bf16[768,1536]{1,0:T(8,128)(2,1)S(1)} %copy-done.9, bf16[384,2048]{1,0:T(8,128)(2,1)S(1)} %get-tuple-element.46, bf16[384,2048]{1,0:T(8,128)(2,1)S(1)} %get-tuple-element.45), kind=kOutput, calls=%fused_computation | convolution fusion | flops 4841275392 | bytes 11796480 | tf_op jit(solution)/shard_map/nd,nk->dk/dot_general | solution.py:415
  45.1 3.9 %collective-permute-start.10 = (bf16[512,1536]{1,0:T(8,128)(2,1)S(1)}, bf16[512,1536]{1,0:T(8,128)(2,1)S(1)}, u32[]{:S(2)}, u32[]{:S(2)}) collective-permute-start(bf16[512,1536]{1,0:T(8,128)(2,1)S(1)} %pad_maximum_fusion.6), channel_id=1, source_target_pairs={{0,96},{8,104},{16,112},{24,120},{32,0},{40,8},{48,16},{56,24},{64... | collective-permute-start | bytes 4718600 | tf_op jit(solution)/shard_map/ppermute | solution.py:29
  50.5 4.7 %convolution_convert_fusion.1 = bf16[2048,1280]{1,0:T(8,128)(2,1)S(1)} fusion(bf16[768,1280]{1,0:T(8,128)(2,1)S(1)} %copy-done.11, bf16[384,2048]{1,0:T(8,128)(2,1)S(1)} %get-tuple-element.46, bf16[384,2048]{1,0:T(8,128)(2,1)S(1)} %get-tuple-element.45), kind=kOutput, calls=%fused_computation.1 | convolution fusion | flops 4035444736 | bytes 10354688 | tf_op jit(solution)/shard_map/nd,nk->dk/dot_general | solution.py:415
  55.8 15.8 %collective-permute-done = bf16[512,2816]{1,0:T(8,128)(2,1)} collective-permute-done((bf16[512,2816]{1,0:T(8,128)(2,1)}, bf16[512,2816]{1,0:T(8,128)(2,1)}, u32[]{:S(2)}, u32[]{:S(2)}) %collective-permute-start) | collective-permute-done | bytes 2883616 | tf_op jit(solution)/shard_map/ppermute | solution.py:24
  77.5 4.2 %convolution_convert_fusion.3 = bf16[768,512]{1,0:T(8,128)(2,1)S(1)} fusion(bf16[768,2816]{1,0:T(8,128)(2,1)S(1)} %bitcast.121, bf16[512,2816]{1,0:T(8,128)(2,1)} %collective-permute-done), kind=kOutput, calls=%fused_computation.21 | convolution fusion | flops 2214985728 | bytes 7995392 | tf_op jit(solution)/shard_map/nk,dk->nd/dot_general | solution.py:475
  81.8 4.2 %convolution_convert_fusion.2 = bf16[768,512]{1,0:T(8,128)(2,1)S(1)} fusion(bf16[768,2816]{1,0:T(8,128)(2,1)S(1)} %bitcast.121, bf16[512,2816]{1,0:T(8,128)(2,1)} %collective-permute-done.1), kind=kOutput, calls=%fused_computation.20 | convolution fusion | flops 2214985728 | bytes 7995392 | tf_op jit(solution)/shard_map/nk,dk->nd/dot_general | solution.py:475
  86.2 17.4 %collective-permute-done.16.refs_1_ = bf16[544,1280]{1,0:T(8,128)(2,1)S(1)} collective-permute-done((bf16[544,1280]{1,0:T(8,128)(2,1)S(1)}, bf16[544,1280]{1,0:T(8,128)(2,1)S(1)}, u32[]{:S(2)}, u32[]{:S(2)}) %collective-permute-start.16) | collective-permute-done | bytes 1392672 | tf_op jit(solution)/shard_map/ppermute | solution.py:29
  108.3 3.6 %collective-permute-start.12 = (bf16[256,1536]{1,0:T(8,128)(2,1)S(1)}, bf16[256,1536]{1,0:T(8,128)(2,1)S(1)}, u32[]{:S(2)}, u32[]{:S(2)}) collective-permute-start(bf16[256,1536]{1,0:T(8,128)(2,1)S(1)} %fusion.2), channel_id=1, source_target_pairs={{0,96},{8,104},{16,112},{24,120},{32,0},{40,8},{48,16},{56,24},{64... | collective-permute-start | bytes 2359304 | tf_op jit(solution)/shard_map/ppermute | solution.py:29
  112.2 7.5 %collective-permute-done.19 = bf16[256,1280]{1,0:T(8,128)(2,1)S(1)} collective-permute-done((bf16[256,1280]{1,0:T(8,128)(2,1)S(1)}, bf16[256,1280]{1,0:T(8,128)(2,1)S(1)}, u32[]{:S(2)}, u32[]{:S(2)}) %collective-permute-start.19) | collective-permute-done | bytes 655392 | tf_op jit(solution)/shard_map/ppermute | solution.py:29
  122.6 3.4 %collective-permute-start.22 = (bf16[160,1280]{1,0:T(8,128)(2,1)S(1)}, bf16[160,1280]{1,0:T(8,128)(2,1)S(1)}, u32[]{:S(2)}, u32[]{:S(2)}) collective-permute-start(bf16[160,1280]{1,0:T(8,128)(2,1)S(1)} %get-tuple-element.72), channel_id=1, source_target_pairs={{0,96},{8,104},{16,112},{24,120},{32,0},{40,8},{48,16},{56,24},{64... | collective-permute-start | bytes 1228808 | tf_op jit(solution)/shard_map/ppermute | solution.py:29
  126.4 11.2 %collective-permute-done.11 = bf16[256,1536]{1,0:T(8,128)(2,1)S(1)} collective-permute-done((bf16[256,1536]{1,0:T(8,128)(2,1)S(1)}, bf16[256,1536]{1,0:T(8,128)(2,1)S(1)}, u32[]{:S(2)}, u32[]{:S(2)}) %collective-permute-start.11) | collective-permute-done | bytes 786464 | tf_op jit(solution)/shard_map/ppermute | solution.py:29
  140.6 5.8 %collective-permute-done.21.refs_1_ = bf16[160,1280]{1,0:T(8,128)(2,1)S(1)} collective-permute-done((bf16[160,1280]{1,0:T(8,128)(2,1)S(1)}, bf16[160,1280]{1,0:T(8,128)(2,1)S(1)}, u32[]{:S(2)}, u32[]{:S(2)}) %collective-permute-start.21) | collective-permute-done | bytes 409632 | tf_op jit(solution)/shard_map/ppermute | solution.py:29
  149.1 7.0 %collective-permute-done.20.refs_3_ = bf16[160,1280]{1,0:T(8,128)(2,1)S(1)} collective-permute-done((bf16[160,1280]{1,0:T(8,128)(2,1)S(1)}, bf16[160,1280]{1,0:T(8,128)(2,1)S(1)}, u32[]{:S(2)}, u32[]{:S(2)}) %collective-permute-start.20) | collective-permute-done | bytes 409632 | tf_op jit(solution)/shard_map/ppermute | solution.py:29
  157.3 3.0 %collective-permute-start.13 = (bf16[128,1536]{1,0:T(8,128)(2,1)S(1)}, bf16[128,1536]{1,0:T(8,128)(2,1)S(1)}, u32[]{:S(2)}, u32[]{:S(2)}) collective-permute-start(bf16[128,1536]{1,0:T(8,128)(2,1)S(1)} %bitcast.142), channel_id=1, source_target_pairs={{0,16},{8,24},{16,0},{24,8},{32,48},{40,56},{48,32},{56,40},{64,80... | collective-permute-start | bytes 1179656 | tf_op jit(solution)/shard_map/ppermute | solution.py:29
  161.6 8.9 %collective-permute-start.5 = (bf16[384,512]{1,0:T(8,128)(2,1)S(1)}, bf16[384,512]{1,0:T(8,128)(2,1)S(1)}, u32[]{:S(2)}, u32[]{:S(2)}) collective-permute-start(bf16[384,512]{1,0:T(8,128)(2,1)S(1)} %get-tuple-element.59), channel_id=1, source_target_pairs={{0,1},{1,0},{2,3},{3,2},{4,5},{5,4},{6,7},{7,6},{8,9},{9,8},{10,11... | collective-permute-start | bytes 1179656 | tf_op jit(solution)/shard_map/ppermute | solution.py:482
  178.2 5.2 %collective-permute-done.24.refs_1_ = bf16[40,2816]{1,0:T(8,128)(2,1)S(1)} collective-permute-done((bf16[40,2816]{1,0:T(8,128)(2,1)S(1)}, bf16[40,2816]{1,0:T(8,128)(2,1)S(1)}, u32[]{:S(2)}, u32[]{:S(2)}) %collective-permute-start.24) | collective-permute-done | bytes 225312 | tf_op jit(solution)/shard_map/ppermute | solution.py:24
  183.5 3.8 %collective-permute-start.34 = (bf16[32,1280]{1,0:T(8,128)(2,1)S(1)}, bf16[32,1280]{1,0:T(8,128)(2,1)S(1)}, u32[]{:S(2)}, u32[]{:S(2)}) collective-permute-start(bf16[32,1280]{1,0:T(8,128)(2,1)S(1)} %slice.215), channel_id=1, source_target_pairs={{0,24},{8,0},{16,8},{24,16},{32,56},{40,32},{48,40},{56,48},{64,88... | collective-permute-start | bytes 245768 | tf_op jit(solution)/shard_map/ppermute | solution.py:29
  195.0 5.2 %collective-permute-start.6 = (bf16[384,512]{1,0:T(8,128)(2,1)S(1)}, bf16[384,512]{1,0:T(8,128)(2,1)S(1)}, u32[]{:S(2)}, u32[]{:S(2)}) collective-permute-start(bf16[384,512]{1,0:T(8,128)(2,1)S(1)} %get-tuple-element.57), channel_id=1, source_target_pairs={{0,1},{1,0},{2,3},{3,2},{4,5},{5,4},{6,7},{7,6},{8,9},{9,8},{10,11... | collective-permute-start | bytes 1179656 | tf_op jit(solution)/shard_map/ppermute | solution.py:482
  211.5 5.0 %collective-permute-done.35.refs_5_ = bf16[4,32,1280]{2,1,0:T(8,128)(2,1)S(1)} collective-permute-done((bf16[4,32,1280]{2,1,0:T(8,128)(2,1)S(1)}, bf16[4,32,1280]{2,1,0:T(8,128)(2,1)S(1)}, u32[]{:S(2)}, u32[]{:S(2)}) %collective-permute-start.35) | collective-permute-done | bytes 327712 | tf_op jit(solution)/shard_map/ppermute | solution.py:29
  218.5 7.9 %collective-permute-done.37.refs_7_ = bf16[4,32,1280]{2,1,0:T(8,128)(2,1)S(1)} collective-permute-done((bf16[4,32,1280]{2,1,0:T(8,128)(2,1)S(1)}, bf16[4,32,1280]{2,1,0:T(8,128)(2,1)S(1)}, u32[]{:S(2)}, u32[]{:S(2)}) %collective-permute-start.37) | collective-permute-done | bytes 327712 | tf_op jit(solution)/shard_map/ppermute | solution.py:29
  226.4 3.3 %finish.1 = (f32[4,4,32,1408]{3,2,1,0:T(8,128)}, f32[4,4,32,1408]{3,2,1,0:T(8,128)}) custom-call(s32[2]{0:T(128)S(1)} %pad_add_fusion.places, bf16[4,32,1536]{2,1,0:T(8,128)(2,1)S(1)} %select_select_fusion.refs_0_, bf16[4,32,1536]{2,1,0:T(8,128)(2,1)S(1)} %collective-permute-done.29.refs_1_, bf16[4,32,1536]{2,1,0:T(8,128)(2,1)S(1)} %collective-permute-done.30.refs_2_, ...), custom_call_target="tpu_custom_call" | custom-call | flops 144179200 | bytes 8650752 | tf_op jit(solution)/shard_map/finish/pallas_call | solution.py:365
  (142 shorter events, 71.0 us)
Async XLA Ops:
  5.7 65.9 %collective-permute-start = (bf16[512,2816]{1,0:T(8,128)(2,1)}, bf16[512,2816]{1,0:T(8,128)(2,1)}, u32[]{:S(2)}, u32[]{:S(2)}) collective-permute-start(bf16[512,2816]{1,0:T(8,128)(2,1)} %weave.1), channel_id=1, source_target_pairs={{0,2},{2,4},{4,6},{6,0},{1,3},{3,5},{5,7},{7,1},{8,10},{10,12},{12... | collective-permute-start | bytes 8650760 | tf_op jit(solution)/shard_map/ppermute | solution.py:24
  7.8 66.4 %collective-permute-start.1 = (bf16[512,2816]{1,0:T(8,128)(2,1)}, bf16[512,2816]{1,0:T(8,128)(2,1)}, u32[]{:S(2)}, u32[]{:S(2)}) collective-permute-start(bf16[512,2816]{1,0:T(8,128)(2,1)} %weave.1), channel_id=1, source_target_pairs={{0,6},{2,0},{4,2},{6,4},{1,7},{3,1},{5,3},{7,5},{8,14},{10,8},{12,... | collective-permute-start | bytes 8650760 | tf_op jit(solution)/shard_map/ppermute | solution.py:24
  9.3 26.8 %collective-permute-start.8 = (bf16[384,2048]{1,0:T(8,128)(2,1)}, bf16[384,2048]{1,0:T(8,128)(2,1)}, u32[]{:S(2)}, u32[]{:S(2)}) collective-permute-start(bf16[384,2048]{1,0:T(8,128)(2,1)} %bitcast.8), channel_id=1, source_target_pairs={{0,1},{1,0},{2,3},{3,2},{4,5},{5,4},{6,7},{7,6},{8,9},{9,8},{10,11... | collective-permute-start | bytes 4718600 | tf_op jit(solution)/shard_map/ppermute | solution.py:398
  35.6 170.3 %collective-permute-start.4 = (bf16[384,512]{1,0:T(8,128)(2,1)S(1)}, bf16[384,512]{1,0:T(8,128)(2,1)S(1)}, u32[]{:S(2)}, u32[]{:S(2)}) collective-permute-start(bf16[384,512]{1,0:T(8,128)(2,1)S(1)} %get-tuple-element.61), channel_id=1, source_target_pairs={{0,1},{1,0},{2,3},{3,2},{4,5},{5,4},{6,7},{7,6},{8,9},{9,8},{10,11... | collective-permute-start | bytes 1179656 | tf_op jit(solution)/shard_map/ppermute | solution.py:482
  45.1 61.2 %collective-permute-start.10 = (bf16[512,1536]{1,0:T(8,128)(2,1)S(1)}, bf16[512,1536]{1,0:T(8,128)(2,1)S(1)}, u32[]{:S(2)}, u32[]{:S(2)}) collective-permute-start(bf16[512,1536]{1,0:T(8,128)(2,1)S(1)} %pad_maximum_fusion.6), channel_id=1, source_target_pairs={{0,96},{8,104},{16,112},{24,120},{32,0},{40,8},{48,16},{56,24},{64... | collective-permute-start | bytes 4718600 | tf_op jit(solution)/shard_map/ppermute | solution.py:29
  49.1 59.2 %collective-permute-start.9 = (bf16[512,1536]{1,0:T(8,128)(2,1)S(1)}, bf16[512,1536]{1,0:T(8,128)(2,1)S(1)}, u32[]{:S(2)}, u32[]{:S(2)}) collective-permute-start(bf16[512,1536]{1,0:T(8,128)(2,1)S(1)} %pad_maximum_fusion.5), channel_id=1, source_target_pairs={{0,32},{8,40},{16,48},{24,56},{32,64},{40,72},{48,80},{56,88},{64,... | collective-permute-start | bytes 4718600 | tf_op jit(solution)/shard_map/ppermute | solution.py:29
  71.7 31.9 %collective-permute-start.16 = (bf16[544,1280]{1,0:T(8,128)(2,1)S(1)}, bf16[544,1280]{1,0:T(8,128)(2,1)S(1)}, u32[]{:S(2)}, u32[]{:S(2)}) collective-permute-start(bf16[544,1280]{1,0:T(8,128)(2,1)S(1)} %get-tuple-element.74), channel_id=1, source_target_pairs={{0,8},{8,16},{16,24},{24,0},{32,40},{40,48},{48,56},{56,32},{64,72... | collective-permute-start | bytes 4177928 | tf_op jit(solution)/shard_map/ppermute | solution.py:29
  74.2 30.6 %collective-permute-start.17 = (bf16[544,1280]{1,0:T(8,128)(2,1)S(1)}, bf16[544,1280]{1,0:T(8,128)(2,1)S(1)}, u32[]{:S(2)}, u32[]{:S(2)}) collective-permute-start(bf16[544,1280]{1,0:T(8,128)(2,1)S(1)} %get-tuple-element.73), channel_id=1, source_target_pairs={{0,24},{8,0},{16,8},{24,16},{32,56},{40,32},{48,40},{56,48},{64,88... | collective-permute-start | bytes 4177928 | tf_op jit(solution)/shard_map/ppermute | solution.py:29
  103.6 53.7 %collective-permute-start.2 = (bf16[256,2816]{1,0:T(8,128)(2,1)S(1)}, bf16[256,2816]{1,0:T(8,128)(2,1)S(1)}, u32[]{:S(2)}, u32[]{:S(2)}) collective-permute-start(bf16[256,2816]{1,0:T(8,128)(2,1)S(1)} %slice.200), channel_id=1, source_target_pairs={{0,2},{2,4},{4,6},{6,0},{1,3},{3,5},{5,7},{7,1},{8,10},{10,12},{12... | collective-permute-start | bytes 4325384 | tf_op jit(solution)/shard_map/ppermute | solution.py:24
  104.8 17.1 %collective-permute-start.18 = (bf16[288,1280]{1,0:T(8,128)(2,1)S(1)}, bf16[288,1280]{1,0:T(8,128)(2,1)S(1)}, u32[]{:S(2)}, u32[]{:S(2)}) collective-permute-start(bf16[288,1280]{1,0:T(8,128)(2,1)S(1)} %pad_maximum_fusion.9), channel_id=1, source_target_pairs={{0,8},{8,16},{16,24},{24,0},{32,40},{40,48},{48,56},{56,32},{64,72... | collective-permute-start | bytes 2211848 | tf_op jit(solution)/shard_map/ppermute | solution.py:29
  106.2 13.5 %collective-permute-start.19 = (bf16[256,1280]{1,0:T(8,128)(2,1)S(1)}, bf16[256,1280]{1,0:T(8,128)(2,1)S(1)}, u32[]{:S(2)}, u32[]{:S(2)}) collective-permute-start(bf16[256,1280]{1,0:T(8,128)(2,1)S(1)} %fusion.8), channel_id=1, source_target_pairs={{0,24},{8,0},{16,8},{24,16},{32,56},{40,32},{48,40},{56,48},{64,88... | collective-permute-start | bytes 1966088 | tf_op jit(solution)/shard_map/ppermute | solution.py:29
  108.3 17.7 %collective-permute-start.12 = (bf16[256,1536]{1,0:T(8,128)(2,1)S(1)}, bf16[256,1536]{1,0:T(8,128)(2,1)S(1)}, u32[]{:S(2)}, u32[]{:S(2)}) collective-permute-start(bf16[256,1536]{1,0:T(8,128)(2,1)S(1)} %fusion.2), channel_id=1, source_target_pairs={{0,96},{8,104},{16,112},{24,120},{32,0},{40,8},{48,16},{56,24},{64... | collective-permute-start | bytes 2359304 | tf_op jit(solution)/shard_map/ppermute | solution.py:29
  119.7 17.9 %collective-permute-start.11 = (bf16[256,1536]{1,0:T(8,128)(2,1)S(1)}, bf16[256,1536]{1,0:T(8,128)(2,1)S(1)}, u32[]{:S(2)}, u32[]{:S(2)}) collective-permute-start(bf16[256,1536]{1,0:T(8,128)(2,1)S(1)} %fusion.3), channel_id=1, source_target_pairs={{0,32},{8,40},{16,48},{24,56},{32,64},{40,72},{48,80},{56,88},{64,... | collective-permute-start | bytes 2359304 | tf_op jit(solution)/shard_map/ppermute | solution.py:29
  122.6 16.7 %collective-permute-start.22 = (bf16[160,1280]{1,0:T(8,128)(2,1)S(1)}, bf16[160,1280]{1,0:T(8,128)(2,1)S(1)}, u32[]{:S(2)}, u32[]{:S(2)}) collective-permute-start(bf16[160,1280]{1,0:T(8,128)(2,1)S(1)} %get-tuple-element.72), channel_id=1, source_target_pairs={{0,96},{8,104},{16,112},{24,120},{32,0},{40,8},{48,16},{56,24},{64... | collective-permute-start | bytes 1228808 | tf_op jit(solution)/shard_map/ppermute | solution.py:29
  126.0 20.5 %collective-permute-start.21 = (bf16[160,1280]{1,0:T(8,128)(2,1)S(1)}, bf16[160,1280]{1,0:T(8,128)(2,1)S(1)}, u32[]{:S(2)}, u32[]{:S(2)}) collective-permute-start(bf16[160,1280]{1,0:T(8,128)(2,1)S(1)} %get-tuple-element.71), channel_id=1, source_target_pairs={{0,32},{8,40},{16,48},{24,56},{32,64},{40,72},{48,80},{56,88},{64,... | collective-permute-start | bytes 1228808 | tf_op jit(solution)/shard_map/ppermute | solution.py:29
  137.7 18.5 %collective-permute-start.20 = (bf16[160,1280]{1,0:T(8,128)(2,1)S(1)}, bf16[160,1280]{1,0:T(8,128)(2,1)S(1)}, u32[]{:S(2)}, u32[]{:S(2)}) collective-permute-start(bf16[160,1280]{1,0:T(8,128)(2,1)S(1)} %get-tuple-element.70), channel_id=1, source_target_pairs={{0,64},{8,72},{16,80},{24,88},{32,96},{40,104},{48,112},{56,120},{... | collective-permute-start | bytes 1228808 | tf_op jit(solution)/shard_map/ppermute | solution.py:29
  139.3 35.7 %collective-permute-start.3 = (bf16[256,2816]{1,0:T(8,128)(2,1)S(1)}, bf16[256,2816]{1,0:T(8,128)(2,1)S(1)}, u32[]{:S(2)}, u32[]{:S(2)}) collective-permute-start(bf16[256,2816]{1,0:T(8,128)(2,1)S(1)} %slice.201), channel_id=1, source_target_pairs={{0,6},{2,0},{4,2},{6,4},{1,7},{3,1},{5,3},{7,5},{8,14},{10,8},{12,... | collective-permute-start | bytes 4325384 | tf_op jit(solution)/shard_map/ppermute | solution.py:24
  146.4 15.2 %collective-permute-start.15 = (bf16[128,1536]{1,0:T(8,128)(2,1)S(1)}, bf16[128,1536]{1,0:T(8,128)(2,1)S(1)}, u32[]{:S(2)}, u32[]{:S(2)}) collective-permute-start(bf16[128,1536]{1,0:T(8,128)(2,1)S(1)} %bitcast.144), channel_id=1, source_target_pairs={{0,24},{8,0},{16,8},{24,16},{32,56},{40,32},{48,40},{56,48},{64,88... | collective-permute-start | bytes 1179656 | tf_op jit(solution)/shard_map/ppermute | solution.py:29
  156.1 14.4 %collective-permute-start.14 = (bf16[128,1536]{1,0:T(8,128)(2,1)S(1)}, bf16[128,1536]{1,0:T(8,128)(2,1)S(1)}, u32[]{:S(2)}, u32[]{:S(2)}) collective-permute-start(bf16[128,1536]{1,0:T(8,128)(2,1)S(1)} %bitcast.143), channel_id=1, source_target_pairs={{0,8},{8,16},{16,24},{24,0},{32,40},{40,48},{48,56},{56,32},{64,72... | collective-permute-start | bytes 1179656 | tf_op jit(solution)/shard_map/ppermute | solution.py:29
  157.3 15.4 %collective-permute-start.13 = (bf16[128,1536]{1,0:T(8,128)(2,1)S(1)}, bf16[128,1536]{1,0:T(8,128)(2,1)S(1)}, u32[]{:S(2)}, u32[]{:S(2)}) collective-permute-start(bf16[128,1536]{1,0:T(8,128)(2,1)S(1)} %bitcast.142), channel_id=1, source_target_pairs={{0,16},{8,24},{16,0},{24,8},{32,48},{40,56},{48,32},{56,40},{64,80... | collective-permute-start | bytes 1179656 | tf_op jit(solution)/shard_map/ppermute | solution.py:29
  161.6 44.4 %collective-permute-start.5 = (bf16[384,512]{1,0:T(8,128)(2,1)S(1)}, bf16[384,512]{1,0:T(8,128)(2,1)S(1)}, u32[]{:S(2)}, u32[]{:S(2)}) collective-permute-start(bf16[384,512]{1,0:T(8,128)(2,1)S(1)} %get-tuple-element.59), channel_id=1, source_target_pairs={{0,1},{1,0},{2,3},{3,2},{4,5},{5,4},{6,7},{7,6},{8,9},{9,8},{10,11... | collective-permute-start | bytes 1179656 | tf_op jit(solution)/shard_map/ppermute | solution.py:482
  206.0 20.4 %collective-permute-start.29 = (bf16[4,32,1536]{2,1,0:T(8,128)(2,1)S(1)}, bf16[4,32,1536]{2,1,0:T(8,128)(2,1)S(1)}, u32[]{:S(2)}, u32[]{:S(2)}) collective-permute-start(bf16[4,32,1536]{2,1,0:T(8,128)(2,1)S(1)} %select_select_fusion.refs_0_), channel_id=1, source_target_pairs={{0,8},{8,16},{16,24},{24,0},{32,40},{40,48},{48,56},{56,32},{64,72... | collective-permute-start | bytes 1179656 | tf_op jit(solution)/shard_map/ppermute | solution.py:29
  206.1 20.3 %collective-permute-start.30 = (bf16[4,32,1536]{2,1,0:T(8,128)(2,1)S(1)}, bf16[4,32,1536]{2,1,0:T(8,128)(2,1)S(1)}, u32[]{:S(2)}, u32[]{:S(2)}) collective-permute-start(bf16[4,32,1536]{2,1,0:T(8,128)(2,1)S(1)} %select_select_fusion.refs_0_), channel_id=1, source_target_pairs={{0,24},{8,0},{16,8},{24,16},{32,56},{40,32},{48,40},{56,48},{64,88... | collective-permute-start | bytes 1179656 | tf_op jit(solution)/shard_map/ppermute | solution.py:29
  208.8 17.6 %collective-permute-start.31 = (bf16[4,32,1536]{2,1,0:T(8,128)(2,1)S(1)}, bf16[4,32,1536]{2,1,0:T(8,128)(2,1)S(1)}, u32[]{:S(2)}, u32[]{:S(2)}) collective-permute-start(bf16[4,32,1536]{2,1,0:T(8,128)(2,1)S(1)} %select_select_fusion.refs_0_), channel_id=1, source_target_pairs={{0,16},{8,24},{16,0},{24,8},{32,48},{40,56},{48,32},{56,40},{64,80... | collective-permute-start | bytes 1179656 | tf_op jit(solution)/shard_map/ppermute | solution.py:29
  (29 other events, 209.3 us)

commit v3 on v2

--- a/solution.py
+++ b/solution.py
@@ -256,7 +256,9 @@
             bytes_accessed=length * LANES * blocks * 14,
             transcendentals=length * LANES * blocks,
         ),
-        compiler_params=pltpu.CompilerParams(vmem_limit_bytes=16 * 1024 * 1024),
+        compiler_params=pltpu.CompilerParams(
+            vmem_limit_bytes=(16 if first else 58) * 1024 * 1024
+        ),
         name="backward",
     )(*operands)
 
@@ -280,7 +282,6 @@
         cost_estimate=pl.CostEstimate(
             flops=100 * rows * columns, bytes_accessed=8 * rows * columns, transcendentals=0
         ),
-        compiler_params=pltpu.CompilerParams(vmem_limit_bytes=8 * 1024 * 1024),
         name="weave",
     )(gate, up)
 

time: 231 us -> 230 us (level)
  waiting for transfers between devices: 91.1 us -> 87.1 us
  Pallas kernels: 21.7 us -> 25.5 us
    ppermute x7, waiting for transfers between devices: 21.7 us -> 17.8 us  [shift(): return lax.ppermute(value, 'fs', [(i, (i + hop) % SIDE) for i in ring])]
  transfers between devices with their start and end apart: 39 -> 39, of which waited for: 15 -> 15; matrix products, arithmetic and copies ran while one was open for 17% -> 16% of each run, Pallas kernels for 7% -> 8%
where the time goes in v3:
time: 230 us; the launch traced here: 229 us
  waiting for transfers between devices  87.1 us (38%)
  starting transfers between devices  67.8 us (29%)
  matrix products  25.9 us (11%)
  Pallas kernels  25.5 us (11%)
  local copies, waits for them, and re-layouts  14.1 us (6%)
  other arithmetic  7 us (3%)
    ppermute x26, waiting for transfers between devices, shift(): return lax.ppermute(value, 'rep', pairs)  69.3 us
    ppermute x26, starting transfers between devices, shift(): return lax.ppermute(value, 'rep', pairs)  39.1 us
    ppermute x7, waiting for transfers between devices, shift(): return lax.ppermute(value, 'fs', [(i, (i + hop) % SIDE) for i in ring])  17.8 us
    ppermute x4, starting transfers between devices, layer(): got = [lax.ppermute(p, 'tp', swap) for p in away]  16.9 us
    pallas_call x2, Pallas kernels, backward(): pl.pallas_call(backward_kernel, grid_spec=pltpu.PrefetchScalarGridSpec(nu...  16.5 us
    dot_general x5, matrix products, project(): jnp.einsum('nk,dk->nd', stacked, w, preferred_element_type=jnp.float32)  15.7 us
    dot_general x2, matrix products, layer(): jnp.einsum('nd,nk->dk', whole_rows, group, preferred_element_type=jnp.flo...  10.2 us
    unnamed x28, local copies, waits for them, and re-layouts  9.5 us
  transfers between devices with their start and end apart: 39, of which 15 were waited for; matrix products, arithmetic and copies ran while one was open for 16% of the time, Pallas kernels for 8%

profile of v3, /device:TPU:1, one launch (start us, length us, event | category | flops | bytes accessed | tf_op | source)
XLA Modules:
  0.0 229.0 jit_solution(4672556791269975878)
XLA Ops:
  0.6 4.2 %weave.1 = bf16[512,2816]{1,0:T(8,128)(2,1)} custom-call(bf16[512,1408]{1,0:T(8,128)(2,1)} %gate_ref.1, bf16[512,1408]{1,0:T(8,128)(2,1)} %up_ref.1), custom_call_target="tpu_custom_call" | custom-call | flops 72089600 | bytes 5767168 | tf_op jit(solution)/shard_map/weave/pallas_call | solution.py:276
  9.5 9.8 %backward.2 = (bf16[768,1536]{1,0:T(8,128)(2,1)}, bf16[768,2816]{1,0:T(8,128)(2,1)}, f32[8,768]{1,0:T(8,128)}) custom-call(s32[1]{0:T(128)} %bitcast.1.tp_ref, bf16[768,1408]{1,0:T(8,128)(2,1)} %bitcast.114, bf16[768,1408]{1,0:T(8,128)(2,1)} %bitcast.116, bf16[768,1408]{1,0:T(8,128)(2,1)} %bitcast.118, bf16[3,2816]{1,0:T(4,128)(2,1)} %tap_gate_ref.3, ...), custom_call_target="tpu_custom_call" | custom-call | flops 1179648000 | bytes 8257536 | tf_op jit(solution)/shard_map/backward/pallas_call | solution.py:235
  23.2 6.7 %backward.3 = (bf16[768,1280]{1,0:T(8,128)(2,1)S(1)}, bf16[768,2816]{1,0:T(8,128)(2,1)S(1)}, f32[8,640]{1,0:T(8,128)S(1)}) custom-call(s32[1]{0:T(128)} %bitcast.1.tp_ref, bf16[768,1408]{1,0:T(8,128)(2,1)S(1)} %bitcast.115, bf16[768,1408]{1,0:T(8,128)(2,1)S(1)} %bitcast.117, bf16[768,1408]{1,0:T(8,128)(2,1)S(1)} %bitcast.119, ...), custom_call_target="tpu_custom_call", output_to_operand_aliasing={{1}: (6, {})} | custom-call | flops 983040000 | bytes 6881280 | tf_op jit(solution)/shard_map/backward/pallas_call | solution.py:235
  33.3 4.6 %convolution_convert_fusion.4 = bf16[768,512]{1,0:T(8,128)(2,1)S(1)} fusion(bf16[768,2816]{1,0:T(8,128)(2,1)} %copy-done.4, bf16[512,2816]{1,0:T(8,128)(2,1)S(1)} %copy-done.10), kind=kOutput, calls=%fused_computation.22 | convolution fusion | flops 2214985728 | bytes 7995392 | tf_op jit(solution)/shard_map/nk,dk->nd/dot_general | solution.py:476
  41.7 5.5 %convolution_convert_fusion = bf16[2048,1536]{1,0:T(8,128)(2,1)S(1)} fusion(bf16[768,1536]{1,0:T(8,128)(2,1)S(1)} %copy-done.11, bf16[384,2048]{1,0:T(8,128)(2,1)S(1)} %get-tuple-element.46, bf16[384,2048]{1,0:T(8,128)(2,1)S(1)} %get-tuple-element.45), kind=kOutput, calls=%fused_computation | convolution fusion | flops 4841275392 | bytes 11796480 | tf_op jit(solution)/shard_map/nd,nk->dk/dot_general | solution.py:416
  48.0 3.9 %collective-permute-start.10 = (bf16[512,1536]{1,0:T(8,128)(2,1)S(1)}, bf16[512,1536]{1,0:T(8,128)(2,1)S(1)}, u32[]{:S(2)}, u32[]{:S(2)}) collective-permute-start(bf16[512,1536]{1,0:T(8,128)(2,1)S(1)} %pad_maximum_fusion.6), channel_id=1, source_target_pairs={{0,96},{8,104},{16,112},{24,120},{32,0},{40,8},{48,16},{56,24},{64... | collective-permute-start | bytes 4718600 | tf_op jit(solution)/shard_map/ppermute | solution.py:29
  53.5 4.7 %convolution_convert_fusion.1 = bf16[2048,1280]{1,0:T(8,128)(2,1)S(1)} fusion(bf16[768,1280]{1,0:T(8,128)(2,1)S(1)} %copy-done.9, bf16[384,2048]{1,0:T(8,128)(2,1)S(1)} %get-tuple-element.46, bf16[384,2048]{1,0:T(8,128)(2,1)S(1)} %get-tuple-element.45), kind=kOutput, calls=%fused_computation.1 | convolution fusion | flops 4035444736 | bytes 10354688 | tf_op jit(solution)/shard_map/nd,nk->dk/dot_general | solution.py:416
  58.9 11.9 %collective-permute-done = bf16[512,2816]{1,0:T(8,128)(2,1)} collective-permute-done((bf16[512,2816]{1,0:T(8,128)(2,1)}, bf16[512,2816]{1,0:T(8,128)(2,1)}, u32[]{:S(2)}, u32[]{:S(2)}) %collective-permute-start) | collective-permute-done | bytes 2883616 | tf_op jit(solution)/shard_map/ppermute | solution.py:24
  76.7 4.2 %convolution_convert_fusion.3 = bf16[768,512]{1,0:T(8,128)(2,1)S(1)} fusion(bf16[768,2816]{1,0:T(8,128)(2,1)S(1)} %bitcast.121, bf16[512,2816]{1,0:T(8,128)(2,1)} %collective-permute-done), kind=kOutput, calls=%fused_computation.21 | convolution fusion | flops 2214985728 | bytes 7995392 | tf_op jit(solution)/shard_map/nk,dk->nd/dot_general | solution.py:476
  80.9 4.2 %convolution_convert_fusion.2 = bf16[768,512]{1,0:T(8,128)(2,1)S(1)} fusion(bf16[768,2816]{1,0:T(8,128)(2,1)S(1)} %bitcast.121, bf16[512,2816]{1,0:T(8,128)(2,1)} %collective-permute-done.1), kind=kOutput, calls=%fused_computation.20 | convolution fusion | flops 2214985728 | bytes 7995392 | tf_op jit(solution)/shard_map/nk,dk->nd/dot_general | solution.py:476
  85.3 17.4 %collective-permute-done.16.refs_1_ = bf16[544,1280]{1,0:T(8,128)(2,1)S(1)} collective-permute-done((bf16[544,1280]{1,0:T(8,128)(2,1)S(1)}, bf16[544,1280]{1,0:T(8,128)(2,1)S(1)}, u32[]{:S(2)}, u32[]{:S(2)}) %collective-permute-start.16) | collective-permute-done | bytes 1392672 | tf_op jit(solution)/shard_map/ppermute | solution.py:29
  107.4 3.6 %collective-permute-start.12 = (bf16[256,1536]{1,0:T(8,128)(2,1)S(1)}, bf16[256,1536]{1,0:T(8,128)(2,1)S(1)}, u32[]{:S(2)}, u32[]{:S(2)}) collective-permute-start(bf16[256,1536]{1,0:T(8,128)(2,1)S(1)} %fusion.2), channel_id=1, source_target_pairs={{0,96},{8,104},{16,112},{24,120},{32,0},{40,8},{48,16},{56,24},{64... | collective-permute-start | bytes 2359304 | tf_op jit(solution)/shard_map/ppermute | solution.py:29
  111.3 7.5 %collective-permute-done.19 = bf16[256,1280]{1,0:T(8,128)(2,1)S(1)} collective-permute-done((bf16[256,1280]{1,0:T(8,128)(2,1)S(1)}, bf16[256,1280]{1,0:T(8,128)(2,1)S(1)}, u32[]{:S(2)}, u32[]{:S(2)}) %collective-permute-start.19) | collective-permute-done | bytes 655392 | tf_op jit(solution)/shard_map/ppermute | solution.py:29
  121.7 3.4 %collective-permute-start.22 = (bf16[160,1280]{1,0:T(8,128)(2,1)S(1)}, bf16[160,1280]{1,0:T(8,128)(2,1)S(1)}, u32[]{:S(2)}, u32[]{:S(2)}) collective-permute-start(bf16[160,1280]{1,0:T(8,128)(2,1)S(1)} %get-tuple-element.72), channel_id=1, source_target_pairs={{0,96},{8,104},{16,112},{24,120},{32,0},{40,8},{48,16},{56,24},{64... | collective-permute-start | bytes 1228808 | tf_op jit(solution)/shard_map/ppermute | solution.py:29
  125.6 11.2 %collective-permute-done.11 = bf16[256,1536]{1,0:T(8,128)(2,1)S(1)} collective-permute-done((bf16[256,1536]{1,0:T(8,128)(2,1)S(1)}, bf16[256,1536]{1,0:T(8,128)(2,1)S(1)}, u32[]{:S(2)}, u32[]{:S(2)}) %collective-permute-start.11) | collective-permute-done | bytes 786464 | tf_op jit(solution)/shard_map/ppermute | solution.py:29
  139.7 5.8 %collective-permute-done.21.refs_1_ = bf16[160,1280]{1,0:T(8,128)(2,1)S(1)} collective-permute-done((bf16[160,1280]{1,0:T(8,128)(2,1)S(1)}, bf16[160,1280]{1,0:T(8,128)(2,1)S(1)}, u32[]{:S(2)}, u32[]{:S(2)}) %collective-permute-start.21) | collective-permute-done | bytes 409632 | tf_op jit(solution)/shard_map/ppermute | solution.py:29
  148.3 7.0 %collective-permute-done.20.refs_3_ = bf16[160,1280]{1,0:T(8,128)(2,1)S(1)} collective-permute-done((bf16[160,1280]{1,0:T(8,128)(2,1)S(1)}, bf16[160,1280]{1,0:T(8,128)(2,1)S(1)}, u32[]{:S(2)}, u32[]{:S(2)}) %collective-permute-start.20) | collective-permute-done | bytes 409632 | tf_op jit(solution)/shard_map/ppermute | solution.py:29
  160.8 8.9 %collective-permute-start.5 = (bf16[384,512]{1,0:T(8,128)(2,1)S(1)}, bf16[384,512]{1,0:T(8,128)(2,1)S(1)}, u32[]{:S(2)}, u32[]{:S(2)}) collective-permute-start(bf16[384,512]{1,0:T(8,128)(2,1)S(1)} %get-tuple-element.59), channel_id=1, source_target_pairs={{0,1},{1,0},{2,3},{3,2},{4,5},{5,4},{6,7},{7,6},{8,9},{9,8},{10,11... | collective-permute-start | bytes 1179656 | tf_op jit(solution)/shard_map/ppermute | solution.py:483
  177.4 5.2 %collective-permute-done.24.refs_1_ = bf16[40,2816]{1,0:T(8,128)(2,1)S(1)} collective-permute-done((bf16[40,2816]{1,0:T(8,128)(2,1)S(1)}, bf16[40,2816]{1,0:T(8,128)(2,1)S(1)}, u32[]{:S(2)}, u32[]{:S(2)}) %collective-permute-start.24) | collective-permute-done | bytes 225312 | tf_op jit(solution)/shard_map/ppermute | solution.py:24
  182.7 3.8 %collective-permute-start.34 = (bf16[32,1280]{1,0:T(8,128)(2,1)S(1)}, bf16[32,1280]{1,0:T(8,128)(2,1)S(1)}, u32[]{:S(2)}, u32[]{:S(2)}) collective-permute-start(bf16[32,1280]{1,0:T(8,128)(2,1)S(1)} %slice.215), channel_id=1, source_target_pairs={{0,24},{8,0},{16,8},{24,16},{32,56},{40,32},{48,40},{56,48},{64,88... | collective-permute-start | bytes 245768 | tf_op jit(solution)/shard_map/ppermute | solution.py:29
  194.2 5.2 %collective-permute-start.6 = (bf16[384,512]{1,0:T(8,128)(2,1)S(1)}, bf16[384,512]{1,0:T(8,128)(2,1)S(1)}, u32[]{:S(2)}, u32[]{:S(2)}) collective-permute-start(bf16[384,512]{1,0:T(8,128)(2,1)S(1)} %get-tuple-element.57), channel_id=1, source_target_pairs={{0,1},{1,0},{2,3},{3,2},{4,5},{5,4},{6,7},{7,6},{8,9},{9,8},{10,11... | collective-permute-start | bytes 1179656 | tf_op jit(solution)/shard_map/ppermute | solution.py:483
  210.6 5.0 %collective-permute-done.35.refs_5_ = bf16[4,32,1280]{2,1,0:T(8,128)(2,1)S(1)} collective-permute-done((bf16[4,32,1280]{2,1,0:T(8,128)(2,1)S(1)}, bf16[4,32,1280]{2,1,0:T(8,128)(2,1)S(1)}, u32[]{:S(2)}, u32[]{:S(2)}) %collective-permute-start.35) | collective-permute-done | bytes 327712 | tf_op jit(solution)/shard_map/ppermute | solution.py:29
  217.6 7.9 %collective-permute-done.37.refs_7_ = bf16[4,32,1280]{2,1,0:T(8,128)(2,1)S(1)} collective-permute-done((bf16[4,32,1280]{2,1,0:T(8,128)(2,1)S(1)}, bf16[4,32,1280]{2,1,0:T(8,128)(2,1)S(1)}, u32[]{:S(2)}, u32[]{:S(2)}) %collective-permute-start.37) | collective-permute-done | bytes 327712 | tf_op jit(solution)/shard_map/ppermute | solution.py:29
  225.6 3.3 %finish.1 = (f32[4,4,32,1408]{3,2,1,0:T(8,128)}, f32[4,4,32,1408]{3,2,1,0:T(8,128)}) custom-call(s32[2]{0:T(128)S(1)} %pad_add_fusion.places, bf16[4,32,1536]{2,1,0:T(8,128)(2,1)S(1)} %select_select_fusion.refs_0_, bf16[4,32,1536]{2,1,0:T(8,128)(2,1)S(1)} %collective-permute-done.29.refs_1_, bf16[4,32,1536]{2,1,0:T(8,128)(2,1)S(1)} %collective-permute-done.30.refs_2_, ...), custom_call_target="tpu_custom_call" | custom-call | flops 144179200 | bytes 8650752 | tf_op jit(solution)/shard_map/finish/pallas_call | solution.py:366
  (142 shorter events, 72.3 us)
Async XLA Ops:
  4.8 65.9 %collective-permute-start = (bf16[512,2816]{1,0:T(8,128)(2,1)}, bf16[512,2816]{1,0:T(8,128)(2,1)}, u32[]{:S(2)}, u32[]{:S(2)}) collective-permute-start(bf16[512,2816]{1,0:T(8,128)(2,1)} %weave.1), channel_id=1, source_target_pairs={{0,2},{2,4},{4,6},{6,0},{1,3},{3,5},{5,7},{7,1},{8,10},{10,12},{12... | collective-permute-start | bytes 8650760 | tf_op jit(solution)/shard_map/ppermute | solution.py:24
  7.0 66.4 %collective-permute-start.1 = (bf16[512,2816]{1,0:T(8,128)(2,1)}, bf16[512,2816]{1,0:T(8,128)(2,1)}, u32[]{:S(2)}, u32[]{:S(2)}) collective-permute-start(bf16[512,2816]{1,0:T(8,128)(2,1)} %weave.1), channel_id=1, source_target_pairs={{0,6},{2,0},{4,2},{6,4},{1,7},{3,1},{5,3},{7,5},{8,14},{10,8},{12,... | collective-permute-start | bytes 8650760 | tf_op jit(solution)/shard_map/ppermute | solution.py:24
  8.4 30.7 %collective-permute-start.8 = (bf16[384,2048]{1,0:T(8,128)(2,1)}, bf16[384,2048]{1,0:T(8,128)(2,1)}, u32[]{:S(2)}, u32[]{:S(2)}) collective-permute-start(bf16[384,2048]{1,0:T(8,128)(2,1)} %bitcast.8), channel_id=1, source_target_pairs={{0,1},{1,0},{2,3},{3,2},{4,5},{5,4},{6,7},{7,6},{8,9},{9,8},{10,11... | collective-permute-start | bytes 4718600 | tf_op jit(solution)/shard_map/ppermute | solution.py:399
  38.0 167.1 %collective-permute-start.4 = (bf16[384,512]{1,0:T(8,128)(2,1)S(1)}, bf16[384,512]{1,0:T(8,128)(2,1)S(1)}, u32[]{:S(2)}, u32[]{:S(2)}) collective-permute-start(bf16[384,512]{1,0:T(8,128)(2,1)S(1)} %get-tuple-element.61), channel_id=1, source_target_pairs={{0,1},{1,0},{2,3},{3,2},{4,5},{5,4},{6,7},{7,6},{8,9},{9,8},{10,11... | collective-permute-start | bytes 1179656 | tf_op jit(solution)/shard_map/ppermute | solution.py:483
  48.0 57.4 %collective-permute-start.10 = (bf16[512,1536]{1,0:T(8,128)(2,1)S(1)}, bf16[512,1536]{1,0:T(8,128)(2,1)S(1)}, u32[]{:S(2)}, u32[]{:S(2)}) collective-permute-start(bf16[512,1536]{1,0:T(8,128)(2,1)S(1)} %pad_maximum_fusion.6), channel_id=1, source_target_pairs={{0,96},{8,104},{16,112},{24,120},{32,0},{40,8},{48,16},{56,24},{64... | collective-permute-start | bytes 4718600 | tf_op jit(solution)/shard_map/ppermute | solution.py:29
  52.1 55.4 %collective-permute-start.9 = (bf16[512,1536]{1,0:T(8,128)(2,1)S(1)}, bf16[512,1536]{1,0:T(8,128)(2,1)S(1)}, u32[]{:S(2)}, u32[]{:S(2)}) collective-permute-start(bf16[512,1536]{1,0:T(8,128)(2,1)S(1)} %pad_maximum_fusion.5), channel_id=1, source_target_pairs={{0,32},{8,40},{16,48},{24,56},{32,64},{40,72},{48,80},{56,88},{64,... | collective-permute-start | bytes 4718600 | tf_op jit(solution)/shard_map/ppermute | solution.py:29
  70.8 31.9 %collective-permute-start.16 = (bf16[544,1280]{1,0:T(8,128)(2,1)S(1)}, bf16[544,1280]{1,0:T(8,128)(2,1)S(1)}, u32[]{:S(2)}, u32[]{:S(2)}) collective-permute-start(bf16[544,1280]{1,0:T(8,128)(2,1)S(1)} %get-tuple-element.74), channel_id=1, source_target_pairs={{0,8},{8,16},{16,24},{24,0},{32,40},{40,48},{48,56},{56,32},{64,72... | collective-permute-start | bytes 4177928 | tf_op jit(solution)/shard_map/ppermute | solution.py:29
  73.4 30.6 %collective-permute-start.17 = (bf16[544,1280]{1,0:T(8,128)(2,1)S(1)}, bf16[544,1280]{1,0:T(8,128)(2,1)S(1)}, u32[]{:S(2)}, u32[]{:S(2)}) collective-permute-start(bf16[544,1280]{1,0:T(8,128)(2,1)S(1)} %get-tuple-element.73), channel_id=1, source_target_pairs={{0,24},{8,0},{16,8},{24,16},{32,56},{40,32},{48,40},{56,48},{64,88... | collective-permute-start | bytes 4177928 | tf_op jit(solution)/shard_map/ppermute | solution.py:29
  102.7 53.7 %collective-permute-start.2 = (bf16[256,2816]{1,0:T(8,128)(2,1)S(1)}, bf16[256,2816]{1,0:T(8,128)(2,1)S(1)}, u32[]{:S(2)}, u32[]{:S(2)}) collective-permute-start(bf16[256,2816]{1,0:T(8,128)(2,1)S(1)} %slice.200), channel_id=1, source_target_pairs={{0,2},{2,4},{4,6},{6,0},{1,3},{3,5},{5,7},{7,1},{8,10},{10,12},{12... | collective-permute-start | bytes 4325384 | tf_op jit(solution)/shard_map/ppermute | solution.py:24
  103.9 17.1 %collective-permute-start.18 = (bf16[288,1280]{1,0:T(8,128)(2,1)S(1)}, bf16[288,1280]{1,0:T(8,128)(2,1)S(1)}, u32[]{:S(2)}, u32[]{:S(2)}) collective-permute-start(bf16[288,1280]{1,0:T(8,128)(2,1)S(1)} %pad_maximum_fusion.9), channel_id=1, source_target_pairs={{0,8},{8,16},{16,24},{24,0},{32,40},{40,48},{48,56},{56,32},{64,72... | collective-permute-start | bytes 2211848 | tf_op jit(solution)/shard_map/ppermute | solution.py:29
  105.4 13.5 %collective-permute-start.19 = (bf16[256,1280]{1,0:T(8,128)(2,1)S(1)}, bf16[256,1280]{1,0:T(8,128)(2,1)S(1)}, u32[]{:S(2)}, u32[]{:S(2)}) collective-permute-start(bf16[256,1280]{1,0:T(8,128)(2,1)S(1)} %fusion.8), channel_id=1, source_target_pairs={{0,24},{8,0},{16,8},{24,16},{32,56},{40,32},{48,40},{56,48},{64,88... | collective-permute-start | bytes 1966088 | tf_op jit(solution)/shard_map/ppermute | solution.py:29
  107.4 17.6 %collective-permute-start.12 = (bf16[256,1536]{1,0:T(8,128)(2,1)S(1)}, bf16[256,1536]{1,0:T(8,128)(2,1)S(1)}, u32[]{:S(2)}, u32[]{:S(2)}) collective-permute-start(bf16[256,1536]{1,0:T(8,128)(2,1)S(1)} %fusion.2), channel_id=1, source_target_pairs={{0,96},{8,104},{16,112},{24,120},{32,0},{40,8},{48,16},{56,24},{64... | collective-permute-start | bytes 2359304 | tf_op jit(solution)/shard_map/ppermute | solution.py:29
  118.9 17.9 %collective-permute-start.11 = (bf16[256,1536]{1,0:T(8,128)(2,1)S(1)}, bf16[256,1536]{1,0:T(8,128)(2,1)S(1)}, u32[]{:S(2)}, u32[]{:S(2)}) collective-permute-start(bf16[256,1536]{1,0:T(8,128)(2,1)S(1)} %fusion.3), channel_id=1, source_target_pairs={{0,32},{8,40},{16,48},{24,56},{32,64},{40,72},{48,80},{56,88},{64,... | collective-permute-start | bytes 2359304 | tf_op jit(solution)/shard_map/ppermute | solution.py:29
  121.7 16.7 %collective-permute-start.22 = (bf16[160,1280]{1,0:T(8,128)(2,1)S(1)}, bf16[160,1280]{1,0:T(8,128)(2,1)S(1)}, u32[]{:S(2)}, u32[]{:S(2)}) collective-permute-start(bf16[160,1280]{1,0:T(8,128)(2,1)S(1)} %get-tuple-element.72), channel_id=1, source_target_pairs={{0,96},{8,104},{16,112},{24,120},{32,0},{40,8},{48,16},{56,24},{64... | collective-permute-start | bytes 1228808 | tf_op jit(solution)/shard_map/ppermute | solution.py:29
  125.1 20.5 %collective-permute-start.21 = (bf16[160,1280]{1,0:T(8,128)(2,1)S(1)}, bf16[160,1280]{1,0:T(8,128)(2,1)S(1)}, u32[]{:S(2)}, u32[]{:S(2)}) collective-permute-start(bf16[160,1280]{1,0:T(8,128)(2,1)S(1)} %get-tuple-element.71), channel_id=1, source_target_pairs={{0,32},{8,40},{16,48},{24,56},{32,64},{40,72},{48,80},{56,88},{64,... | collective-permute-start | bytes 1228808 | tf_op jit(solution)/shard_map/ppermute | solution.py:29
  136.8 18.5 %collective-permute-start.20 = (bf16[160,1280]{1,0:T(8,128)(2,1)S(1)}, bf16[160,1280]{1,0:T(8,128)(2,1)S(1)}, u32[]{:S(2)}, u32[]{:S(2)}) collective-permute-start(bf16[160,1280]{1,0:T(8,128)(2,1)S(1)} %get-tuple-element.70), channel_id=1, source_target_pairs={{0,64},{8,72},{16,80},{24,88},{32,96},{40,104},{48,112},{56,120},{... | collective-permute-start | bytes 1228808 | tf_op jit(solution)/shard_map/ppermute | solution.py:29
  138.4 35.7 %collective-permute-start.3 = (bf16[256,2816]{1,0:T(8,128)(2,1)S(1)}, bf16[256,2816]{1,0:T(8,128)(2,1)S(1)}, u32[]{:S(2)}, u32[]{:S(2)}) collective-permute-start(bf16[256,2816]{1,0:T(8,128)(2,1)S(1)} %slice.201), channel_id=1, source_target_pairs={{0,6},{2,0},{4,2},{6,4},{1,7},{3,1},{5,3},{7,5},{8,14},{10,8},{12,... | collective-permute-start | bytes 4325384 | tf_op jit(solution)/shard_map/ppermute | solution.py:24
  145.6 15.2 %collective-permute-start.15 = (bf16[128,1536]{1,0:T(8,128)(2,1)S(1)}, bf16[128,1536]{1,0:T(8,128)(2,1)S(1)}, u32[]{:S(2)}, u32[]{:S(2)}) collective-permute-start(bf16[128,1536]{1,0:T(8,128)(2,1)S(1)} %bitcast.144), channel_id=1, source_target_pairs={{0,24},{8,0},{16,8},{24,16},{32,56},{40,32},{48,40},{56,48},{64,88... | collective-permute-start | bytes 1179656 | tf_op jit(solution)/shard_map/ppermute | solution.py:29
  155.3 14.4 %collective-permute-start.14 = (bf16[128,1536]{1,0:T(8,128)(2,1)S(1)}, bf16[128,1536]{1,0:T(8,128)(2,1)S(1)}, u32[]{:S(2)}, u32[]{:S(2)}) collective-permute-start(bf16[128,1536]{1,0:T(8,128)(2,1)S(1)} %bitcast.143), channel_id=1, source_target_pairs={{0,8},{8,16},{16,24},{24,0},{32,40},{40,48},{48,56},{56,32},{64,72... | collective-permute-start | bytes 1179656 | tf_op jit(solution)/shard_map/ppermute | solution.py:29
  156.4 15.4 %collective-permute-start.13 = (bf16[128,1536]{1,0:T(8,128)(2,1)S(1)}, bf16[128,1536]{1,0:T(8,128)(2,1)S(1)}, u32[]{:S(2)}, u32[]{:S(2)}) collective-permute-start(bf16[128,1536]{1,0:T(8,128)(2,1)S(1)} %bitcast.142), channel_id=1, source_target_pairs={{0,16},{8,24},{16,0},{24,8},{32,48},{40,56},{48,32},{56,40},{64,80... | collective-permute-start | bytes 1179656 | tf_op jit(solution)/shard_map/ppermute | solution.py:29
  160.8 44.4 %collective-permute-start.5 = (bf16[384,512]{1,0:T(8,128)(2,1)S(1)}, bf16[384,512]{1,0:T(8,128)(2,1)S(1)}, u32[]{:S(2)}, u32[]{:S(2)}) collective-permute-start(bf16[384,512]{1,0:T(8,128)(2,1)S(1)} %get-tuple-element.59), channel_id=1, source_target_pairs={{0,1},{1,0},{2,3},{3,2},{4,5},{5,4},{6,7},{7,6},{8,9},{9,8},{10,11... | collective-permute-start | bytes 1179656 | tf_op jit(solution)/shard_map/ppermute | solution.py:483
  205.2 20.4 %collective-permute-start.29 = (bf16[4,32,1536]{2,1,0:T(8,128)(2,1)S(1)}, bf16[4,32,1536]{2,1,0:T(8,128)(2,1)S(1)}, u32[]{:S(2)}, u32[]{:S(2)}) collective-permute-start(bf16[4,32,1536]{2,1,0:T(8,128)(2,1)S(1)} %select_select_fusion.refs_0_), channel_id=1, source_target_pairs={{0,8},{8,16},{16,24},{24,0},{32,40},{40,48},{48,56},{56,32},{64,72... | collective-permute-start | bytes 1179656 | tf_op jit(solution)/shard_map/ppermute | solution.py:29
  205.3 20.3 %collective-permute-start.30 = (bf16[4,32,1536]{2,1,0:T(8,128)(2,1)S(1)}, bf16[4,32,1536]{2,1,0:T(8,128)(2,1)S(1)}, u32[]{:S(2)}, u32[]{:S(2)}) collective-permute-start(bf16[4,32,1536]{2,1,0:T(8,128)(2,1)S(1)} %select_select_fusion.refs_0_), channel_id=1, source_target_pairs={{0,24},{8,0},{16,8},{24,16},{32,56},{40,32},{48,40},{56,48},{64,88... | collective-permute-start | bytes 1179656 | tf_op jit(solution)/shard_map/ppermute | solution.py:29
  207.9 17.6 %collective-permute-start.31 = (bf16[4,32,1536]{2,1,0:T(8,128)(2,1)S(1)}, bf16[4,32,1536]{2,1,0:T(8,128)(2,1)S(1)}, u32[]{:S(2)}, u32[]{:S(2)}) collective-permute-start(bf16[4,32,1536]{2,1,0:T(8,128)(2,1)S(1)} %select_select_fusion.refs_0_), channel_id=1, source_target_pairs={{0,16},{8,24},{16,0},{24,8},{32,48},{40,56},{48,32},{56,40},{64,80... | collective-permute-start | bytes 1179656 | tf_op jit(solution)/shard_map/ppermute | solution.py:29
  (29 other events, 215.5 us)
